TPU v7x, 32 devices: a whole 2x2x4 slice. The times are simulated.
32 devices in a mesh: sp: 4 (over y, x), dp: 8 (over z, core).
Axes of the slice: x: 2, y: 2, z: 4, core: 2. Of those that a mesh axis runs over, the one named last changes fastest.
Arguments:
- tokens: bfloat16 [8, 1024, 2048], P('dp', 'sp'), may hold values from -6 to 6
- in_gain: float32 [2048], replicated, may hold values from 0.1 to 1.9
- query_weight: bfloat16 [2048, 2048], P('dp'), may hold values from -1 to 1
- key_weight: bfloat16 [2048, 512], P('dp'), may hold values from -1 to 1
- value_matrix: bfloat16 [2048, 512], P('dp'), may hold values from -0.125 to 0.125
- query_gain: float32 [128], replicated, may hold values from 1 to 6
- key_gain: float32 [128], replicated, may hold values from 1 to 6
- out_weight: bfloat16 [2048, 2048], P('dp'), may hold values from -0.125 to 0.125
- out_gain: float32 [2048], replicated, may hold values from 0.1 to 1.9
Outputs:
- mixed: bfloat16 [8, 1024, 2048], P('dp', 'sp')
All inputs are finite; a program needn't handle non-finite values.
Results may differ from a plain program's by a relative error of at most 0.0055.
The roundings to bfloat16 on the way count: a program that leaves them out, or rounds other values in their place, can miss the bound.
Values may be sent and summed in bfloat16 or wider, within the bound.
A program may use at most 128 MiB of HBM per device.

v0:
```python
import functools

import jax
import jax.numpy as jnp
import numpy as np
from jax import lax
from jax.experimental import pallas as pl
from jax.experimental.pallas import tpu as pltpu
from jax.sharding import PartitionSpec as P

QUERY_HEAD_COUNT = 16
KEY_VALUE_HEADS = 4
HEAD_WIDTH = 128
GRID_W = 64
EPS = 1e-06
THETA = 10000.0
MESH = pl.DeviceIdType.MESH
ANY = pl.BlockSpec(memory_space=pl.ANY)


def remote(src, dst, send_sem, recv_sem, device):
    return pltpu.make_async_remote_copy(
        src_ref=src, dst_ref=dst, send_sem=send_sem, recv_sem=recv_sem,
        device_id=device, device_id_type=MESH,
    )


def gather_kernel(
    parts, chips, q_width, kv_width, first_kv_of,
    x_ref, wq_ref, wk_ref, wv_ref, wo_ref, rows_ref, cols_ref, head_ref, tail_ref,
    stage, x_send, x_recv, own_sem, stage_sem,
    up_send, up_recv, down_send, down_recv, pair_send, pair_recv,
):
    sp, dp = lax.axis_index("sp"), lax.axis_index("dp")
    z, core = dp // 2, dp % 2
    partner = z * 2 + (1 - core)
    row_count = x_ref.shape[0]
    depth = stage.shape[0]
    square = parts == 4

    first_kv = first_kv_of(sp)
    loads = [
        pltpu.make_async_copy(
            wq_ref.at[:, pl.ds(pl.multiple_of(sp * q_width, 128), q_width)],
            stage.at[:, pl.ds(0, q_width)], stage_sem.at[0]),
        pltpu.make_async_copy(
            wk_ref.at[:, pl.ds(pl.multiple_of(first_kv * HEAD_WIDTH, 128), kv_width)],
            stage.at[:, pl.ds(q_width, kv_width)], stage_sem.at[1]),
        pltpu.make_async_copy(
            wv_ref.at[:, pl.ds(pl.multiple_of(first_kv * HEAD_WIDTH, 128), kv_width)],
            stage.at[:, pl.ds(q_width + kv_width, kv_width)], stage_sem.at[2]),
    ]
    for load in loads:
        load.start()

    barrier = pltpu.get_barrier_semaphore()
    if square:
        x_side = (sp // 2) * 2 + (1 - sp % 2)
        y_side = (1 - sp // 2) * 2 + sp % 2
        corner = (1 - sp // 2) * 2 + (1 - sp % 2)
        greeted = [x_side, y_side]
    else:
        greeted = [lax.rem(sp + i, parts) for i in range(1, parts)]
    for peer in greeted:
        pl.semaphore_signal(barrier, inc=1, device_id={"sp": peer, "dp": dp}, device_id_type=MESH)
    pl.semaphore_signal(barrier, inc=1, device_id={"sp": sp, "dp": partner}, device_id_type=MESH)

    @pl.when(z < chips - 1)
    def _():
        pl.semaphore_signal(barrier, inc=1, device_id={"sp": sp, "dp": dp + 2}, device_id_type=MESH)

    @pl.when(z > 0)
    def _():
        pl.semaphore_signal(barrier, inc=1, device_id={"sp": sp, "dp": dp - 2}, device_id_type=MESH)

    in_chain = (z + chips - 1) // chips + (2 * chips - 2 - z) // chips
    pl.semaphore_wait(barrier, len(greeted) + 1 + in_chain)

    def token_rows(owner, half=None):
        if half is None:
            return rows_ref.at[pl.ds(owner * row_count, row_count)]
        return rows_ref.at[pl.ds(owner * row_count + half * (row_count // 2), row_count // 2)]

    token_sends = []
    if square:
        for half_x, half_y in ((0, 1), (1, 0)):
            for slot, half, peer in ((0, half_x, x_side), (1, half_y, y_side)):
                copy = remote(
                    x_ref.at[pl.ds(half * (row_count // 2), row_count // 2)],
                    token_rows(sp, half), x_send.at[slot * 2 + half],
                    x_recv.at[slot * 2 + half], {"sp": peer, "dp": dp})
                copy.start()
                token_sends.append(copy)
    else:
        for i, peer in enumerate(greeted):
            copy = remote(
                x_ref, token_rows(sp), x_send.at[i], x_recv.at[i], {"sp": peer, "dp": dp})
            copy.start()
            token_sends.append(copy)
    own_rows = pltpu.make_async_copy(x_ref, token_rows(sp), own_sem.at[0])
    own_rows.start()
    split = head_ref.shape[1]
    out_head = wo_ref.at[:, pl.ds(0, split)]
    own_tail = pltpu.make_async_copy(
        wo_ref.at[:, pl.ds(split, tail_ref.shape[1])], tail_ref, own_sem.at[2])
    own_tail.start()

    for load in loads:
        load.wait()

    gathered = (cols_ref, head_ref)
    sources = (stage, out_head)

    def block(t, owner_z, owner_core):
        return gathered[t].at[pl.ds((owner_z * 2 + owner_core) * depth, depth)]

    def to_up(t, src, k):
        return remote(src, block(t, z - k, core), up_send.at[t, k], up_recv.at[t, k + 1],
                      {"sp": sp, "dp": dp + 2})

    def to_down(t, src, k):
        return remote(src, block(t, z + k, core), down_send.at[t, k], down_recv.at[t, k + 1],
                      {"sp": sp, "dp": dp - 2})

    def to_pair(t, src, owner_z):
        return remote(src, block(t, owner_z, core), pair_send.at[t, owner_z],
                      pair_recv.at[t, owner_z], {"sp": sp, "dp": partner})

    own_copies = []
    for t in range(2):
        @pl.when(z < chips - 1)
        def _():
            to_up(t, sources[t], 0).start()

        @pl.when(z > 0)
        def _():
            to_down(t, sources[t], 0).start()

        to_pair(t, sources[t], z).start()
        own = pltpu.make_async_copy(sources[t], block(t, z, core), own_sem.at[(1, 3)[t]])
        own.start()
        own_copies.append(own)

    if square:
        got_x = remote(x_ref.at[pl.ds(0, row_count // 2)], token_rows(x_side, 0),
                       x_send.at[0], x_recv.at[0], {"sp": x_side, "dp": dp})
        got_y = remote(x_ref.at[pl.ds(0, row_count // 2)], token_rows(y_side, 1),
                       x_send.at[3], x_recv.at[3], {"sp": y_side, "dp": dp})

    def relay_columns(t, k):
        @pl.when(z >= k)
        def _():
            source = block(t, z - k, core)
            remote(source, source, up_send.at[t, k], up_recv.at[t, k],
                   {"sp": sp, "dp": partner}).wait_recv()
            if k < chips - 1:
                @pl.when(z < chips - 1)
                def _():
                    to_up(t, source, k).start()
            to_pair(t, source, z - k).start()

        @pl.when(z + k <= chips - 1)
        def _():
            source = block(t, z + k, core)
            remote(source, source, down_send.at[t, k], down_recv.at[t, k],
                   {"sp": sp, "dp": partner}).wait_recv()
            if k < chips - 1:
                @pl.when(z > 0)
                def _():
                    to_down(t, source, k).start()
            to_pair(t, source, z + k).start()

    if chips > 1:
        relay_columns(0, 1)
    if square:
        got_x.wait_recv()
        relay_x = remote(token_rows(x_side, 0), token_rows(x_side, 0),
                         x_send.at[4], x_recv.at[4], {"sp": y_side, "dp": dp})
        relay_x.start()
        got_y.wait_recv()
        relay_y = remote(token_rows(y_side, 1), token_rows(y_side, 1),
                         x_send.at[5], x_recv.at[5], {"sp": x_side, "dp": dp})
        relay_y.start()
        token_sends += [relay_x, relay_y]
    for k in range(1, chips):
        if k > 1:
            relay_columns(0, k)
        relay_columns(1, k)

    for t in range(2):
        for owner_z in range(chips):
            source = block(t, owner_z, 1 - core)
            remote(source, source, pair_send.at[t, owner_z], pair_recv.at[t, owner_z],
                   {"sp": sp, "dp": partner}).wait_recv()
    if square:
        for owner, half, slot in (
            (x_side, 1, 1), (y_side, 0, 2), (corner, 0, 4), (corner, 1, 5)
        ):
            target = token_rows(owner, half)
            remote(target, target, x_send.at[slot], x_recv.at[slot],
                   {"sp": x_side, "dp": dp}).wait_recv()
    else:
        for i in range(parts - 1):
            target = token_rows(lax.rem(sp + parts - 1 - i, parts))
            remote(target, target, x_send.at[i], x_recv.at[i],
                   {"sp": greeted[0], "dp": dp}).wait_recv()
    for copy in token_sends:
        copy.wait_send()
    for t in range(2):
        for owner_z in range(chips):
            to_pair(t, sources[t], owner_z).wait_send()
        for k in range(chips - 1):
            @pl.when(jnp.logical_and(z < chips - 1, z >= k))
            def _():
                to_up(t, sources[t], k).wait_send()

            @pl.when(jnp.logical_and(z > 0, z + k <= chips - 1))
            def _():
                to_down(t, sources[t], k).wait_send()
    own_rows.wait()
    own_tail.wait()
    for own in own_copies:
        own.wait()


def gather(sequence, query_weight, key_weight, value_matrix, out_weight, parts, chips, q_width, kv_width, first_kv_of):
    depth, width = query_weight.shape[0], q_width + 2 * kv_width
    row_count, features = sequence.shape
    dma = pltpu.SemaphoreType.DMA
    chain = dma((2, chips + 1))
    split = out_weight.shape[1] // 2
    return pl.pallas_call(
        functools.partial(gather_kernel, parts, chips, q_width, kv_width, first_kv_of),
        out_shape=(
            jax.ShapeDtypeStruct((parts * row_count, features), jnp.bfloat16),
            jax.ShapeDtypeStruct((chips * 2 * depth, width), jnp.bfloat16),
            jax.ShapeDtypeStruct((chips * 2 * depth, split), jnp.bfloat16),
            jax.ShapeDtypeStruct((depth, out_weight.shape[1] - split), jnp.bfloat16),
        ),
        in_specs=[pl.BlockSpec(memory_space=pltpu.VMEM), ANY, ANY, ANY,
                  pl.BlockSpec(memory_space=pltpu.VMEM)],
        out_specs=(ANY, ANY, ANY, ANY),
        scratch_shapes=[
            pltpu.VMEM((depth, width), jnp.bfloat16),
            dma((max(6, parts),)), dma((max(6, parts),)), dma((4,)), dma((3,)),
            chain, chain, chain, chain, chain, chain,
        ],
        compiler_params=pltpu.CompilerParams(collective_id=0, has_side_effects=True),
        cost_estimate=pl.CostEstimate(flops=40_000_000_000, bytes_accessed=100_000_000, transcendentals=0),
        name="gather_rows_columns",
    )(sequence, query_weight, key_weight, value_matrix, out_weight)


def exchange_kernel(parts, a_ref, o_ref, send, recv, own_sem):
    sp, dp = lax.axis_index("sp"), lax.axis_index("dp")
    row_count = o_ref.shape[1]
    barrier = pltpu.get_barrier_semaphore()
    peers = [lax.rem(sp + i, parts) for i in range(1, parts)]
    for peer in peers:
        pl.semaphore_signal(barrier, inc=1, device_id={"sp": peer, "dp": dp}, device_id_type=MESH)
    pl.semaphore_wait(barrier, parts - 1)
    copies = []
    for i, peer in enumerate(peers):
        copy = remote(a_ref.at[pl.ds(peer * row_count, row_count)], o_ref.at[sp],
                      send.at[i], recv.at[i], {"sp": peer, "dp": dp})
        copy.start()
        copies.append(copy)
    own = pltpu.make_async_copy(a_ref.at[pl.ds(sp * row_count, row_count)], o_ref.at[sp], own_sem)
    own.start()
    for i in range(parts - 1):
        target = o_ref.at[lax.rem(sp + parts - 1 - i, parts)]
        remote(target, target, send.at[i], recv.at[i], {"sp": peers[0], "dp": dp}).wait_recv()
    for copy in copies:
        copy.wait_send()
    own.wait()


def exchange(attended, parts):
    length, width = attended.shape
    row_count = length // parts
    dma = pltpu.SemaphoreType.DMA
    return pl.pallas_call(
        functools.partial(exchange_kernel, parts),
        out_shape=jax.ShapeDtypeStruct((parts, row_count, width), jnp.bfloat16),
        in_specs=[pl.BlockSpec(memory_space=pltpu.VMEM)],
        out_specs=ANY,
        scratch_shapes=[dma((parts,)), dma((parts,)), dma],
        compiler_params=pltpu.CompilerParams(collective_id=1, has_side_effects=True),
        cost_estimate=pl.CostEstimate(flops=10_000_000_000, bytes_accessed=20_000_000, transcendentals=0),
        name="exchange_heads",
    )(attended)


def project_kernel(q_heads, kv_heads, x_ref, g_ref, w_ref, qg_ref, kg_ref, cos_ref, sin_ref,
                   q_ref, k_ref, v_ref):
    x = x_ref[...].astype(jnp.float32)
    scale = lax.rsqrt(jnp.mean(x * x, axis=-1, keepdims=True) + EPS)
    normed = (x * scale * g_ref[...]).astype(jnp.bfloat16)
    mixed = jnp.dot(normed, w_ref[...], preferred_element_type=jnp.float32)
    cosine, sine = cos_ref[...], sin_ref[...]
    lane = lax.broadcasted_iota(jnp.int32, cosine.shape, 1)
    first = lane % (HEAD_WIDTH // 2) < HEAD_WIDTH // 4

    def finish(head, gain):
        head = head * lax.rsqrt(jnp.mean(head * head, axis=-1, keepdims=True) + EPS) * gain
        other = jnp.where(first, pltpu.roll(head, HEAD_WIDTH - HEAD_WIDTH // 4, 1),
                          pltpu.roll(head, HEAD_WIDTH // 4, 1))
        return (head * cosine + other * sine).astype(jnp.bfloat16)

    for h in range(q_heads):
        span = slice(h * HEAD_WIDTH, (h + 1) * HEAD_WIDTH)
        q_ref[:, span] = finish(mixed[:, span], qg_ref[...])
    for h in range(kv_heads):
        span = slice(h * HEAD_WIDTH, (h + 1) * HEAD_WIDTH)
        start = (q_heads + h) * HEAD_WIDTH
        k_ref[:, span] = finish(mixed[:, start:start + HEAD_WIDTH], kg_ref[...])
    v_ref[...] = mixed[:, (q_heads + kv_heads) * HEAD_WIDTH:].astype(jnp.bfloat16)


def project(rows, in_gain, columns, query_gain, key_gain, cosine, sine, q_heads, kv_heads, row_block):
    length, features = rows.shape
    width = columns.shape[1]
    q_width, kv_width = q_heads * HEAD_WIDTH, kv_heads * HEAD_WIDTH
    whole = lambda shape: pl.BlockSpec(shape, lambda i: (0, 0))
    part = lambda size: pl.BlockSpec((row_block, size), lambda i: (i, 0))
    return pl.pallas_call(
        functools.partial(project_kernel, q_heads, kv_heads),
        grid=(length // row_block,),
        out_shape=tuple(jax.ShapeDtypeStruct((length, n), jnp.bfloat16) for n in (q_width, kv_width, kv_width)),
        in_specs=[part(features), whole((1, features)), whole((features, width)),
                  whole((1, HEAD_WIDTH)), whole((1, HEAD_WIDTH)), part(HEAD_WIDTH), part(HEAD_WIDTH)],
        out_specs=(part(q_width), part(kv_width), part(kv_width)),
        cost_estimate=pl.CostEstimate(flops=2 * length * features * width, bytes_accessed=9_000_000, transcendentals=0),
        name="project_heads",
    )(rows, in_gain[None], columns, query_gain[None], key_gain[None], cosine, sine)


def attend_kernel(group, q_ref, k_ref, v_ref, o_ref):
    factor = HEAD_WIDTH ** (-0.5) * float(np.log2(np.e))
    for h in range(q_ref.shape[1] // HEAD_WIDTH):
        span = slice(h * HEAD_WIDTH, (h + 1) * HEAD_WIDTH)
        shared = slice(h // group * HEAD_WIDTH, (h // group + 1) * HEAD_WIDTH)
        scores = lax.dot_general(q_ref[:, span], k_ref[:, shared], (((1,), (1,)), ((), ())),
                                 preferred_element_type=jnp.float32)
        top = jnp.max(scores, axis=-1, keepdims=True)
        raised = jnp.exp2((scores - top) * factor)
        weights = (raised * (1.0 / jnp.sum(raised, axis=-1, keepdims=True))).astype(jnp.bfloat16)
        o_ref[:, span] = jnp.dot(
            weights, v_ref[:, shared], preferred_element_type=jnp.float32).astype(jnp.bfloat16)


def attend(q, k, v, q_heads, kv_heads, row_block):
    length = q.shape[0]
    block = pl.BlockSpec((row_block, q.shape[1]), lambda i: (i, 0))
    keys = pl.BlockSpec(k.shape, lambda i: (0, 0))
    return pl.pallas_call(
        functools.partial(attend_kernel, q_heads // kv_heads),
        grid=(length // row_block,),
        out_shape=jax.ShapeDtypeStruct(q.shape, jnp.bfloat16),
        in_specs=[block, keys, keys],
        out_specs=block,
        cost_estimate=pl.CostEstimate(flops=4 * length * length * q_heads * HEAD_WIDTH,
                                      bytes_accessed=3_000_000, transcendentals=length * length * q_heads),
        name="attend_heads",
    )(q, k, v)


def output_kernel(a_ref, head_ref, tail_ref, g_ref, o_ref, total):
    step = pl.program_id(0)
    split = head_ref.shape[1]

    @pl.when(step == 0)
    def _():
        total[...] = jnp.zeros_like(total)

    total[:, :split] += jnp.dot(a_ref[0], head_ref[...], preferred_element_type=jnp.float32)
    total[:, split:] += jnp.dot(a_ref[0], tail_ref[...], preferred_element_type=jnp.float32)

    @pl.when(step == pl.num_programs(0) - 1)
    def _():
        x = total[...]
        scale = lax.rsqrt(jnp.mean(x * x, axis=-1, keepdims=True) + EPS)
        o_ref[...] = (x * scale * g_ref[...]).astype(jnp.bfloat16)


def output(returned, out_head, out_tail, out_gain):
    parts, row_count, width = returned.shape
    features = out_gain.shape[0]
    split = out_head.shape[1]
    return pl.pallas_call(
        output_kernel,
        grid=(parts,),
        out_shape=jax.ShapeDtypeStruct((row_count, features), jnp.bfloat16),
        in_specs=[pl.BlockSpec((1, row_count, width), lambda s: (s, 0, 0)),
                  pl.BlockSpec((width, split), lambda s: (s, 0)),
                  pl.BlockSpec((width, features - split), lambda s: (s, 0)),
                  pl.BlockSpec((1, features), lambda s: (0, 0))],
        out_specs=pl.BlockSpec((row_count, features), lambda s: (0, 0)),
        scratch_shapes=[pltpu.VMEM((row_count, features), jnp.float32)],
        cost_estimate=pl.CostEstimate(flops=2 * row_count * features * width * parts,
                                      bytes_accessed=10_000_000, transcendentals=0),
        name="output_rows",
    )(returned, out_head, out_tail, out_gain[None])


def rotation(length):
    quarter = HEAD_WIDTH // 4
    inverse_freq = (THETA ** (-np.arange(quarter, dtype=np.float32) / quarter)).astype(np.float32)

    def table(count):
        angle = (np.arange(count, dtype=np.float32)[:, None] * inverse_freq[None, :]).astype(np.float64)
        cosine, sine = np.cos(angle), np.sin(angle)
        return (np.concatenate([cosine, cosine], 1).astype(np.float32),
                np.concatenate([-sine, sine], 1).astype(np.float32))

    rows = -(-length // GRID_W)
    row_tables, col_tables = table(rows), table(GRID_W)
    half = HEAD_WIDTH // 2
    out = []
    for row, col in zip(row_tables, col_tables):
        row = np.broadcast_to(row[:, None, :], (rows, GRID_W, half))
        col = np.broadcast_to(col[None, :, :], (rows, GRID_W, half))
        full = np.concatenate([row, col], -1).reshape(rows * GRID_W, HEAD_WIDTH)
        out.append(jnp.asarray(full[:length]))
    return out


def on_device(parts, groups, tokens, in_gain, query_weight, key_weight, value_matrix,
              query_gain, key_gain, out_weight, out_gain):
    sequence = tokens[0]
    row_count = sequence.shape[0]
    q_heads = QUERY_HEAD_COUNT // parts
    kv_heads = max(1, KEY_VALUE_HEADS // parts)
    per_group = QUERY_HEAD_COUNT // KEY_VALUE_HEADS
    cosine, sine = rotation(parts * row_count)
    rows, columns, out_head, own_tail = gather(
        sequence, query_weight, key_weight, value_matrix, out_weight, parts, groups // 2,
        q_heads * HEAD_WIDTH, kv_heads * HEAD_WIDTH, lambda sp: sp * q_heads // per_group)
    out_tail = lax.all_gather(own_tail, "dp", axis=0, tiled=True)
    q, k, v = project(rows, in_gain, columns, query_gain, key_gain, cosine, sine, q_heads, kv_heads, row_count)
    attended = attend(q, k, v, q_heads, kv_heads, row_count)
    returned = exchange(attended, parts)
    return output(returned, out_head, out_tail, out_gain)[None]


def solution(mesh):
    placed = (P("dp", "sp", None), P(), P("dp", None), P("dp", None), P("dp", None),
              P(), P(), P("dp", None), P())
    return jax.shard_map(
        functools.partial(on_device, mesh.shape["sp"], mesh.shape["dp"]),
        mesh=mesh, in_specs=placed, out_specs=P("dp", "sp", None), check_vma=False,
    )
```

profile of v0, /device:TPU:1, one launch (start us, length us, event | category | flops | bytes accessed | tf_op | source)
XLA Modules:
  0.0 135.7 jit_solution(15116989674391109945)
XLA Ops:
  6.5 0.0 all-gather.2.cloned.1.call-start
  6.5 68.2 %gather_rows_columns.1 = (bf16[1024,2048]{1,0:T(8,128)(2,1)}, bf16[2048,768]{1,0:T(8,128)(2,1)}, bf16[2048,1024]{1,0:T(8,128)(2,1)}, bf16[256,1024]{1,0:T(8,128)(2,1)}) custom-call(bf16[256,2048]{1,0:T(8,128)(2,1)} %bitcast.7, bf16[256,2048]{1,0:T(8,128)(2,1)} %wq_ref.1, bf16[256,512]{1,0:T(8,128)(2,1)} %wk_ref.1, bf16[256,512]{1,0:T(8,128)(2,1)} %wv_ref.1, ...), custom_call_target="tpu_custom_call" | custom-call | flops 40000000000 | bytes 100000000 | tf_op jit(solution)/shard_map/gather_rows_columns/pallas_call | solution.py:232
  74.7 0.0 all-gather.2.cloned.1.call-update
  74.7 9.3 %project_heads.1 = (bf16[1024,512]{1,0:T(8,128)(2,1)}, bf16[1024,128]{1,0:T(8,128)(2,1)}, bf16[1024,128]{1,0:T(8,128)(2,1)}) custom-call(bf16[1024,2048]{1,0:T(8,128)(2,1)} %get-tuple-element.12.x_ref, f32[1,2048]{1,0:T(1,128)} %bitcast.8, bf16[2048,768]{1,0:T(8,128)(2,1)} %get-tuple-element.13.w_ref, f32[1,128]{1,0:T(1,128)} %bitcast.9, f32[1,128]{1,0:T(1,128)} %bitcast.10, ...), custom_call_target="tpu_custom_call" | custom-call | flops 3221225472 | bytes 9000000 | tf_op jit(solution)/shard_map/project_heads/pallas_call | solution.py:326
  84.1 12.2 %attend_heads.1.a_ref = bf16[1024,512]{1,0:T(8,128)(2,1)} custom-call(bf16[1024,512]{1,0:T(8,128)(2,1)} %get-tuple-element.14.q_ref, bf16[1024,128]{1,0:T(8,128)(2,1)} %get-tuple-element.15.k_ref, bf16[1024,128]{1,0:T(8,128)(2,1)} %get-tuple-element.16.v_ref), custom_call_target="tpu_custom_call" | custom-call | flops 2147483648 | bytes 3000000 | tf_op jit(solution)/shard_map/attend_heads/pallas_call | solution.py:356
  96.3 16.3 %exchange_heads.1.a_ref = bf16[4,256,512]{2,1,0:T(8,128)(2,1)} custom-call(bf16[1024,512]{1,0:T(8,128)(2,1)} %attend_heads.1.a_ref), custom_call_target="tpu_custom_call" | custom-call | flops 10000000000 | bytes 20000000 | tf_op jit(solution)/shard_map/exchange_heads/pallas_call | solution.py:282
  112.6 9.2 %all-gather.2.cloned.1.call-done.tail_ref = bf16[2048,1024]{1,0:T(8,128)(2,1)} async-done(((bf16[256,1024]{1,0:T(8,128)(2,1)}), bf16[2048,1024]{1,0:T(8,128)(2,1)}) %all-gather.2.cloned.1.call-update) | async-done | bytes 4194320 | tf_op jit(solution)/shard_map/all_gather | solution.py:439
  121.8 7.1 %output_rows.1 = bf16[256,2048]{1,0:T(8,128)(2,1)} custom-call(bf16[4,256,512]{2,1,0:T(8,128)(2,1)} %exchange_heads.1.a_ref, bf16[2048,1024]{1,0:T(8,128)(2,1)} %get-tuple-element.17.head_ref, bf16[2048,1024]{1,0:T(8,128)(2,1)} %all-gather.2.cloned.1.call-done.tail_ref, f32[1,2048]{1,0:T(1,128)} %bitcast.6), custom_call_target="tpu_custom_call" | custom-call | flops 2147483648 | bytes 10000000 | tf_op jit(solution)/shard_map/output_rows/pallas_call | solution.py:390
Async XLA Ops:
  6.5 115.2 %all-gather.2.cloned.1.call-start = ((), (), s32[]{:S(2)}) async-start(), calls=%async_computation | async-start | bytes 4718592 | tf_op jit(solution)/shard_map/all_gather | solution.py:439
Sparse Core Ops, SparseCore 0:
  74.9 46.8 all-gather.1
where the time goes:
time: 136 us
  Pallas kernels  113 us (83%)
  between operations  13.4 us (10%)
  waiting for transfers between devices  9.23 us (7%)
    pallas_call x1, Pallas kernels, gather(): pl.pallas_call(functools.partial(gather_kernel, parts, chips, q_width, kv...  68.2 us
    pallas_call x1, Pallas kernels, exchange(): pl.pallas_call(functools.partial(exchange_kernel, parts), out_shape=jax.S...  16.3 us
    pallas_call x1, Pallas kernels, attend(): pl.pallas_call(functools.partial(attend_kernel, q_heads // kv_heads), gri...  12.2 us
    pallas_call x1, Pallas kernels, project(): pl.pallas_call(functools.partial(project_kernel, q_heads, kv_heads), grid...  9.33 us
    all_gather x1, waiting for transfers between devices, on_device(): out_tail = lax.all_gather(own_tail, 'dp', axis=0, tiled=True)  9.21 us
    pallas_call x1, Pallas kernels, output(): pl.pallas_call(output_kernel, grid=(parts,), out_shape=jax.ShapeDtypeStru...  7.13 us
  transfers between devices with their start and end apart: 1, of which 1 were waited for; matrix products, arithmetic and copies ran while one was open for 0% of the time, Pallas kernels for 28%

commit v1 on v0

--- a/solution.py
+++ b/solution.py
@@ -403,6 +403,404 @@
     )(returned, out_head, out_tail, out_gain[None])
 
 
+def fused_kernel(
+    chips, q_width, kv_width,
+    x_ref, wq_ref, wk_ref, wv_ref, wo_ref, ig_ref, qg_ref, kg_ref, cos_ref, sin_ref, og_ref,
+    o_ref,
+    xn, wkv, wqb, wob, q_buf, kv_buf, att, total, cosb, sinb,
+    load_sem, tok_send, tok_recv, z_own, z_send, z_recv, y_send, y_recv, x_send, x_recv,
+    kv_send, kv_recv, att_send, att_recv, p_send, p_recv,
+):
+    sp, dp = lax.axis_index("sp"), lax.axis_index("dp")
+    z, core = dp // 2, dp % 2
+    yi, xi = sp // 2, sp % 2
+    R, F = x_ref.shape
+    depth = wq_ref.shape[0]
+    OD = wo_ref.shape[1]
+    share = OD * 3 // 16 // 128 * 128
+    rest = OD - 4 * share
+    half = depth // 2
+    width = 2 * q_width
+    per = q_width // HEAD_WIDTH
+    kv_per = kv_width // HEAD_WIDTH
+    x_peer, y_peer = yi * 2 + (1 - xi), (1 - yi) * 2 + xi
+    corner = (1 - yi) * 2 + (1 - xi)
+    X = {"sp": x_peer, "dp": dp}
+    Y = {"sp": y_peer, "dp": dp}
+    PAIR = {"sp": sp, "dp": z * 2 + (1 - core)}
+    others = chips - 1
+
+    loads = []
+
+    def load(src, dst):
+        copy = pltpu.make_async_copy(src, dst, load_sem.at[len(loads)])
+        copy.start()
+        loads.append(copy)
+
+    mine = pl.ds(pl.multiple_of(dp * depth, depth), depth)
+    for j in range(2):
+        at = pl.ds(pl.multiple_of((2 * xi + j) * kv_width, 128), kv_width)
+        load(wk_ref.at[:, at], wkv.at[j, mine, pl.ds(0, kv_width)])
+        load(wv_ref.at[:, at], wkv.at[j, mine, pl.ds(kv_width, kv_width)])
+    for j in range(2):
+        at = pl.ds(pl.multiple_of((2 * xi + j) * q_width, 128), q_width)
+        load(wq_ref.at[:, at], wqb.at[j, mine])
+    load(wo_ref, wob.at[mine])
+    table = pl.ds(pl.multiple_of(yi * 2 * R, R), 2 * R)
+    load(cos_ref.at[table], cosb)
+    load(sin_ref.at[table], sinb)
+
+    barrier = pltpu.get_barrier_semaphore()
+    for peer in (X, Y, PAIR):
+        pl.semaphore_signal(barrier, inc=1, device_id=peer, device_id_type=MESH)
+
+    @pl.when(z < chips - 1)
+    def _():
+        pl.semaphore_signal(barrier, inc=1, device_id={"sp": sp, "dp": dp + 2}, device_id_type=MESH)
+
+    @pl.when(z > 0)
+    def _():
+        pl.semaphore_signal(barrier, inc=1, device_id={"sp": sp, "dp": dp - 2}, device_id_type=MESH)
+
+    in_chain = (z + others) // chips + (2 * others - z) // chips
+    pl.semaphore_wait(barrier, 3 + in_chain)
+
+    pending = []
+
+    def send(ref, sems, recvs, index, peer, dst=None):
+        copy = remote(ref, ref if dst is None else dst, sems.at[index], recvs.at[index], peer)
+        copy.start()
+        pending.append(copy)
+
+    def arrived(ref, recvs, index):
+        remote(ref, ref, p_send.at[0, 0], recvs.at[index], PAIR).wait_recv()
+
+    def rows(owner, of, start=0, size=depth):
+        return pl.ds(pl.multiple_of((owner * 2 + of) * depth, depth) + start, size)
+
+    def quarter(owner, of, who, start=0, size=depth):
+        return wob.at[rows(owner, of, start, size), pl.ds(pl.multiple_of(who * share, 128), share)]
+
+    def block(t, owner, of, j=None):
+        if t == 0:
+            return wkv.at[yi if j is None else j, rows(owner, of)]
+        if t == 1:
+            return wqb.at[yi if j is None else j, rows(owner, of)]
+        if t == 2:
+            return quarter(owner, of, sp)
+        return wob.at[rows(owner, of), pl.ds(4 * share, rest)]
+
+    low = jnp.minimum(z, others - z)
+
+    def owner_of(i):
+        near = (i + 1) // 2
+        paired = z - near if i % 2 else z + near
+        alone = jnp.where(z > others - z, z - (i - low), z + (i - low))
+        return jnp.where(i <= 2 * low, paired, alone)
+
+    owners = [z] + [owner_of(i) for i in range(1, chips)]
+    last_below = jnp.where(z == 0, 0, jnp.where(z <= others - z, 2 * z - 1, others))
+    above = others - z
+    last_above = jnp.where(above == 0, 0, jnp.where(above <= z, 2 * above, others))
+
+    def start_own(t, up, now=None):
+        ok = z < others if up else z > 0
+        if now is not None:
+            ok = jnp.logical_and(ok, (last_below if up else last_above) == now)
+
+        @pl.when(ok)
+        def _():
+            ref = block(t, z, core)
+            remote(ref, ref, z_own.at[t, int(up)], z_recv.at[t, z],
+                   {"sp": sp, "dp": dp + (2 if up else -2)}).start()
+
+    def to_pair(kind, owner, ref):
+        remote(ref, ref, p_send.at[kind, owner], p_recv.at[kind, owner], PAIR).start()
+        pending.append(remote(ref, ref, p_send.at[kind, owner], p_recv.at[kind, owner], PAIR))
+
+    def relay_target(owner):
+        step = jnp.where(owner < z, 1, -1)
+        return jnp.logical_and(z + step >= 0, z + step < chips), {"sp": sp, "dp": dp + 2 * step}
+
+    def from_z(t, i):
+        owner = owners[i]
+        ref = block(t, owner, core)
+        arrived(ref, z_recv, (t, owner))
+        ok, peer = relay_target(owner)
+
+        @pl.when(ok)
+        def _():
+            remote(ref, ref, z_send.at[t, owner], z_recv.at[t, owner], peer).start()
+
+        if t < 3:
+            send(ref, y_send, y_recv, (t, owner), Y)
+        if t == 2:
+            send(ref, x_send, x_recv, (0, owner), X)
+        to_pair(t, owner, ref)
+
+    def from_y(t, i):
+        owner = owners[i]
+        if t < 2:
+            ref = block(t, owner, core, 1 - yi)
+        else:
+            ref = quarter(owner, core, y_peer)
+        arrived(ref, y_recv, (t, owner))
+        if t == 2:
+            send(quarter(owner, core, y_peer, 0, half), x_send, x_recv, (1, owner), X)
+        to_pair(4 + t, owner, ref)
+
+    def from_x(i):
+        owner = owners[i]
+        ref = quarter(owner, core, x_peer)
+        arrived(ref, x_recv, (0, owner))
+        send(quarter(owner, core, x_peer, half, half), y_send, y_recv, (3, owner), Y)
+        to_pair(7, owner, ref)
+
+    def from_corner(i):
+        owner = owners[i]
+        ref = quarter(owner, core, corner, 0, half)
+        arrived(ref, x_recv, (1, owner))
+        to_pair(8, owner, ref)
+        ref = quarter(owner, core, corner, half, half)
+        arrived(ref, y_recv, (3, owner))
+        to_pair(9, owner, ref)
+
+    def pair_has(kind, ref, owner):
+        arrived(ref, p_recv, (kind, owner))
+
+    send(x_ref, tok_send, tok_recv, 0, X, xn.at[pl.ds(pl.multiple_of(xi * R, R), R)])
+    for copy in loads[:4]:
+        copy.wait()
+    start_own(0, True)
+    start_own(0, False)
+    to_pair(0, z, block(0, z, core))
+    to_pair(4, z, block(0, z, core, 1 - yi))
+    for copy in loads[4:6]:
+        copy.wait()
+    start_own(1, True)
+    start_own(1, False)
+    to_pair(1, z, block(1, z, core))
+    to_pair(5, z, block(1, z, core, 1 - yi))
+    for copy in loads[6:]:
+        copy.wait()
+    to_pair(2, z, wob.at[mine])
+
+    def normalize(values, start):
+        x = values.astype(jnp.float32)
+        scale = lax.rsqrt(jnp.mean(x * x, axis=-1, keepdims=True) + EPS)
+        xn[pl.ds(pl.multiple_of(start, R), R)] = (x * scale * ig_ref[...]).astype(jnp.bfloat16)
+
+    def stage_own(t, now):
+        start_own(t, True, now)
+        start_own(t, False, now)
+
+    normalize(x_ref[...], xi * R)
+    stage_own(2, 0)
+    for i in range(1, chips):
+        from_z(0, i)
+        if i > 1:
+            from_y(1, i - 1)
+        from_z(1, i)
+        stage_own(2, i)
+        from_y(0, i)
+
+    lane = lax.broadcasted_iota(jnp.int32, (R, HEAD_WIDTH), 1)
+    first = lane % (HEAD_WIDTH // 2) < HEAD_WIDTH // 4
+
+    def finish(head, gain, cosine, sine):
+        head = head * lax.rsqrt(jnp.mean(head * head, axis=-1, keepdims=True) + EPS) * gain
+        other = jnp.where(first, pltpu.roll(head, HEAD_WIDTH - HEAD_WIDTH // 4, 1),
+                          pltpu.roll(head, HEAD_WIDTH // 4, 1))
+        return (head * cosine + other * sine).astype(jnp.bfloat16)
+
+    def cut(values, h):
+        return values[:, h * HEAD_WIDTH:(h + 1) * HEAD_WIDTH]
+
+    for owner in range(chips):
+        pair_has(0, block(0, owner, 1 - core), owner)
+        pair_has(4, block(0, owner, 1 - core, 1 - yi), owner)
+
+    def keys_values(who):
+        local = pl.ds(pl.multiple_of(who * R, R), R)
+        placed = pl.ds(pl.multiple_of((yi * 2 + who) * R, R), R)
+        cosine, sine = cosb[local], sinb[local]
+        for j in range(2):
+            mixed = jnp.dot(xn[local], wkv[j], preferred_element_type=jnp.float32)
+            for h in range(kv_per):
+                start = j * kv_width + h * HEAD_WIDTH
+                kv_buf[placed, start:start + HEAD_WIDTH] = finish(cut(mixed, h), kg_ref[...], cosine, sine)
+            start = 2 * kv_width + j * kv_width
+            kv_buf[placed, start:start + kv_width] = mixed[:, kv_width:].astype(jnp.bfloat16)
+        return kv_buf.at[placed]
+
+    send(keys_values(xi), kv_send, kv_recv, 0, Y)
+    theirs = xn.at[pl.ds(pl.multiple_of((1 - xi) * R, R), R)]
+    arrived(theirs, tok_recv, 0)
+    normalize(theirs[...], (1 - xi) * R)
+    send(keys_values(1 - xi), kv_send, kv_recv, 1, Y)
+
+    def queries(j):
+        @pl.loop(0, 2)
+        def _(who):
+            local = pl.ds(pl.multiple_of(who * R, R), R)
+            cosine, sine = cosb[local], sinb[local]
+            mixed = jnp.dot(xn[local], wqb[j], preferred_element_type=jnp.float32)
+            for h in range(per):
+                at = pl.ds(pl.multiple_of(j * q_width + h * HEAD_WIDTH, HEAD_WIDTH), HEAD_WIDTH)
+                q_buf[local, at] = finish(cut(mixed, h), qg_ref[...], cosine, sine)
+
+    stage_own(3, 0)
+    from_z(2, 1)
+    stage_own(3, 1)
+    for owner in range(chips):
+        pair_has(1, block(1, owner, 1 - core), owner)
+    queries(yi)
+    for i in range(2, chips):
+        from_z(2, i)
+        stage_own(3, i)
+    from_y(1, others)
+    for owner in range(chips):
+        pair_has(5, block(1, owner, 1 - core, 1 - yi), owner)
+    queries(1 - yi)
+    from_x(1)
+    for who in range(2):
+        at = pl.ds(pl.multiple_of(((1 - yi) * 2 + (who + xi) % 2) * R, R), R)
+        arrived(kv_buf.at[at], kv_recv, who)
+
+    factor = HEAD_WIDTH ** (-0.5) * float(np.log2(np.e))
+    couple = 2
+    steps = 2 * per // couple
+
+    def attend(step):
+        turn = step % steps
+        who = jnp.where(step < steps, 1 - xi, xi)
+        local = pl.ds(pl.multiple_of(who * R, R), R)
+        base = jnp.where(step < steps, 2 * width, xi * width) + turn * couple * HEAD_WIDTH
+        for u in range(couple):
+            head = turn * couple + u
+            group = head // (per // kv_per)
+            k_at = pl.ds(pl.multiple_of(group * HEAD_WIDTH, HEAD_WIDTH), HEAD_WIDTH)
+            v_at = pl.ds(pl.multiple_of(2 * kv_width + group * HEAD_WIDTH, HEAD_WIDTH), HEAD_WIDTH)
+            q_at = pl.ds(pl.multiple_of(head * HEAD_WIDTH, HEAD_WIDTH), HEAD_WIDTH)
+            scores = lax.dot_general(q_buf[local, q_at], kv_buf[:, k_at], (((1,), (1,)), ((), ())),
+                                     preferred_element_type=jnp.float32)
+            top = jnp.max(scores, axis=-1, keepdims=True)
+            raised = jnp.exp2((scores - top) * factor)
+            weights = (raised * (1.0 / jnp.sum(raised, axis=-1, keepdims=True))).astype(jnp.bfloat16)
+            att[:, pl.ds(pl.multiple_of(base + u * HEAD_WIDTH, HEAD_WIDTH), HEAD_WIDTH)] = jnp.dot(
+                weights, kv_buf[:, v_at], preferred_element_type=jnp.float32).astype(jnp.bfloat16)
+
+    def give(turn):
+        size = couple * HEAD_WIDTH
+        src = att.at[:, pl.ds(2 * width + turn * size, size)]
+        dst = att.at[:, pl.ds(pl.multiple_of(xi * width + turn * size, 128), size)]
+        send(src, att_send, att_recv, turn, X, dst)
+
+    last = 2 * steps - 1
+    timed = []
+    for i in range(1, chips):
+        if i > 1:
+            timed.append((2 * i - 3, lambda i=i: from_x(i)))
+        timed.append((3 * i - 1, lambda i=i: from_y(2, i)))
+        timed.append((2 * i + 1, lambda i=i: from_z(3, i)))
+        timed.append((last, lambda i=i: from_corner(i)))
+    work = [[item for when, item in timed if min(when, last) == step] for step in range(2 * steps)]
+
+    for step in range(2 * steps):
+        attend(step)
+        if step < steps:
+            give(step)
+        for item in work[step]:
+            item()
+
+    for turn in range(steps):
+        size = couple * HEAD_WIDTH
+        ref = att.at[:, pl.ds(pl.multiple_of((1 - xi) * width + turn * size, 128), size)]
+        arrived(ref, att_recv, turn)
+    for i in range(chips):
+        owner = owners[i]
+        if i == 0:
+            pair_has(2, wob.at[rows(owner, 1 - core)], owner)
+        else:
+            pair_has(2, quarter(owner, 1 - core, sp), owner)
+            pair_has(6, quarter(owner, 1 - core, y_peer), owner)
+            pair_has(7, quarter(owner, 1 - core, x_peer), owner)
+            pair_has(8, quarter(owner, 1 - core, corner, 0, half), owner)
+            pair_has(9, quarter(owner, 1 - core, corner, half, half), owner)
+            pair_has(3, block(3, owner, 1 - core), owner)
+
+    tile = OD // 4
+
+    @pl.loop(0, 4)
+    def _(n):
+        at = pl.ds(pl.multiple_of(n * tile, 128), tile)
+        total[:, at] = jnp.dot(att[:, :2 * width], wob[:, at], preferred_element_type=jnp.float32)
+
+    x = total[...]
+    scale = lax.rsqrt(jnp.mean(x * x, axis=-1, keepdims=True) + EPS)
+    o_ref[...] = (x * scale * og_ref[...]).astype(jnp.bfloat16)
+
+    for copy in pending:
+        copy.wait_send()
+    for t in range(4):
+        @pl.when(z < others)
+        def _():
+            ref = block(t, z, core)
+            remote(ref, ref, z_own.at[t, 1], z_recv.at[t, z], PAIR).wait_send()
+
+        @pl.when(z > 0)
+        def _():
+            ref = block(t, z, core)
+            remote(ref, ref, z_own.at[t, 0], z_recv.at[t, z], PAIR).wait_send()
+
+        for i in range(1, chips):
+            owner = owners[i]
+            ok, peer = relay_target(owner)
+
+            @pl.when(ok)
+            def _():
+                ref = block(t, owner, core)
+                remote(ref, ref, z_send.at[t, owner], z_recv.at[t, owner], peer).wait_send()
+
+
+def fused(sequence, in_gain, query_weight, key_weight, value_matrix, query_gain, key_gain,
+          out_weight, out_gain, cosine, sine, chips):
+    row_count, features = sequence.shape
+    q_width, kv_width = query_weight.shape[1] // 4, key_weight.shape[1] // 4
+    columns = out_weight.shape[1]
+    dma = pltpu.SemaphoreType.DMA
+    vmem = pl.BlockSpec(memory_space=pltpu.VMEM)
+    bf16, f32 = jnp.bfloat16, jnp.float32
+    steps = q_width // HEAD_WIDTH
+    return pl.pallas_call(
+        functools.partial(fused_kernel, chips, q_width, kv_width),
+        out_shape=jax.ShapeDtypeStruct((row_count, columns), bf16),
+        in_specs=[vmem, ANY, ANY, ANY, ANY, vmem, vmem, vmem, ANY, ANY, vmem],
+        out_specs=vmem,
+        scratch_shapes=[
+            pltpu.VMEM((2 * row_count, features), bf16),
+            pltpu.VMEM((2, features, 2 * kv_width), bf16),
+            pltpu.VMEM((2, features, q_width), bf16),
+            pltpu.VMEM((out_weight.shape[0] * chips * 2, columns), bf16),
+            pltpu.VMEM((2 * row_count, 2 * q_width), bf16),
+            pltpu.VMEM((4 * row_count, 4 * kv_width), bf16),
+            pltpu.VMEM((row_count, 6 * q_width), bf16),
+            pltpu.VMEM((row_count, columns), f32),
+            pltpu.VMEM((2 * row_count, HEAD_WIDTH), f32),
+            pltpu.VMEM((2 * row_count, HEAD_WIDTH), f32),
+            dma((9,)), dma((1,)), dma((1,)), dma((4, 2)), dma((4, chips)), dma((4, chips)),
+            dma((4, chips)), dma((4, chips)), dma((2, chips)), dma((2, chips)),
+            dma((2,)), dma((2,)), dma((steps,)), dma((steps,)),
+            dma((10, chips)), dma((10, chips)),
+        ],
+        compiler_params=pltpu.CompilerParams(
+            collective_id=0, has_side_effects=True, vmem_limit_bytes=60 * 1024 * 1024),
+        cost_estimate=pl.CostEstimate(flops=10_000_000_000, bytes_accessed=10_000_000, transcendentals=0),
+        name="attention_layer",
+    )(sequence, query_weight, key_weight, value_matrix, out_weight, in_gain[None], query_gain[None],
+      key_gain[None], cosine, sine, out_gain[None])
+
+
 def rotation(length):
     quarter = HEAD_WIDTH // 4
     inverse_freq = (THETA ** (-np.arange(quarter, dtype=np.float32) / quarter)).astype(np.float32)
@@ -433,6 +831,9 @@
     kv_heads = max(1, KEY_VALUE_HEADS // parts)
     per_group = QUERY_HEAD_COUNT // KEY_VALUE_HEADS
     cosine, sine = rotation(parts * row_count)
+    if parts == 4:
+        return fused(sequence, in_gain, query_weight, key_weight, value_matrix, query_gain, key_gain,
+                     out_weight, out_gain, cosine, sine, groups // 2)[None]
     rows, columns, out_head, own_tail = gather(
         sequence, query_weight, key_weight, value_matrix, out_weight, parts, groups // 2,
         q_heads * HEAD_WIDTH, kv_heads * HEAD_WIDTH, lambda sp: sp * q_heads // per_group)

time: 136 us -> 88.5 us (0.65)
  Pallas kernels: 113 us -> 86 us
  between operations: 13.4 us -> 0.01 us
  waiting for transfers between devices: 9.23 us -> 0 us
  local copies, waits for them, and re-layouts: 0 us -> 2.3 us
    pallas_call x5 -> x1, Pallas kernels: 113 us -> 86 us  [fused(): pl.pallas_call(functools.partial(fused_kernel, chips, q_width, kv_width),...]
    all_gather x1 -> x0, waiting for transfers between devices: 9.21 us -> none  [on_device(): out_tail = lax.all_gather(own_tail, 'dp', axis=0, tiled=True)]
    unnamed x0 -> x1, local copies, waits for them, and re-layouts: none -> 2.3 us
  transfers between devices with their start and end apart: 1 -> 0, of which waited for: 1 -> 0; matrix products, arithmetic and copies ran while one was open for 0% -> 0% of each run, Pallas kernels for 28% -> 0%
where the time goes in v1:
time: 88.5 us; the launch traced here: 88.3 us
  Pallas kernels  86 us (97%)
  local copies, waits for them, and re-layouts  2.3 us (3%)
    pallas_call x1, Pallas kernels, fused(): pl.pallas_call(functools.partial(fused_kernel, chips, q_width, kv_width),...  86 us
    unnamed x1, local copies, waits for them, and re-layouts  2.3 us

profile of v1, /device:TPU:1, one launch (start us, length us, event | category | flops | bytes accessed | tf_op | source)
XLA Modules:
  0.0 88.3 jit_solution(783779049322903865)
XLA Ops:
  0.0 86.0 %attention_layer.1 = bf16[256,2048]{1,0:T(8,128)(2,1)} custom-call(bf16[256,2048]{1,0:T(8,128)(2,1)} %bitcast.7, bf16[256,2048]{1,0:T(8,128)(2,1)} %wq_ref.1, bf16[256,512]{1,0:T(8,128)(2,1)} %wk_ref.1, bf16[256,512]{1,0:T(8,128)(2,1)} %wv_ref.1, bf16[256,2048]{1,0:T(8,128)(2,1)} %wo_ref.1, f32[1,2048]{1,0:T(1,128)} %bitcast.8, f32[1,128]{1,0:T(1,128)} %bitcast.10, ...), custom_call_target="tpu_custom_call" | custom-call | flops 10000000000 | bytes 10000000 | tf_op jit(solution)/shard_map/attention_layer/pallas_call | solution.py:775
  86.0 2.3 %copy.13 = bf16[1,256,2048]{2,1,0:T(8,128)(2,1)} copy(bf16[1,256,2048]{2,1,0:T(8,128)(2,1)} %bitcast.6) | data formatting | bytes 2097152

commit v2 on v1

--- a/solution.py
+++ b/solution.py
@@ -405,21 +405,20 @@
 
 def fused_kernel(
     chips, q_width, kv_width,
-    x_ref, wq_ref, wk_ref, wv_ref, wo_ref, ig_ref, qg_ref, kg_ref, cos_ref, sin_ref, og_ref,
+    x_in, wq_ref, wk_ref, wv_ref, wo_ref, ig_in, qg_in, kg_in, cos_ref, sin_ref, og_in,
     o_ref,
-    xn, wkv, wqb, wob, q_buf, kv_buf, att, total, cosb, sinb,
+    x_ref, ig_ref, qg_ref, kg_ref, og_ref, xn, wkv, wqb, wob, q_buf, kv_buf, att, total, out, cosb, sinb,
     load_sem, tok_send, tok_recv, z_own, z_send, z_recv, y_send, y_recv, x_send, x_recv,
-    kv_send, kv_recv, att_send, att_recv, p_send, p_recv,
+    kv_send, kv_recv, att_send, att_recv, p_send, p_recv, own_send, own_recv,
 ):
     sp, dp = lax.axis_index("sp"), lax.axis_index("dp")
     z, core = dp // 2, dp % 2
     yi, xi = sp // 2, sp % 2
-    R, F = x_ref.shape
+    R, F = x_in.shape
     depth = wq_ref.shape[0]
     OD = wo_ref.shape[1]
-    share = OD * 3 // 16 // 128 * 128
-    rest = OD - 4 * share
-    half = depth // 2
+    wide, narrow, rest = OD // 8, OD // 16, OD // 4
+    shared = depth // 2
     width = 2 * q_width
     per = q_width // HEAD_WIDTH
     kv_per = kv_width // HEAD_WIDTH
@@ -430,6 +429,18 @@
     PAIR = {"sp": sp, "dp": z * 2 + (1 - core)}
     others = chips - 1
 
+    barrier = pltpu.get_barrier_semaphore()
+    for peer in (X, Y, PAIR):
+        pl.semaphore_signal(barrier, inc=1, device_id=peer, device_id_type=MESH)
+
+    @pl.when(z < chips - 1)
+    def _():
+        pl.semaphore_signal(barrier, inc=1, device_id={"sp": sp, "dp": dp + 2}, device_id_type=MESH)
+
+    @pl.when(z > 0)
+    def _():
+        pl.semaphore_signal(barrier, inc=1, device_id={"sp": sp, "dp": dp - 2}, device_id_type=MESH)
+
     loads = []
 
     def load(src, dst):
@@ -438,6 +449,7 @@
         loads.append(copy)
 
     mine = pl.ds(pl.multiple_of(dp * depth, depth), depth)
+    load(x_in, x_ref)
     for j in range(2):
         at = pl.ds(pl.multiple_of((2 * xi + j) * kv_width, 128), kv_width)
         load(wk_ref.at[:, at], wkv.at[j, mine, pl.ds(0, kv_width)])
@@ -449,46 +461,55 @@
     table = pl.ds(pl.multiple_of(yi * 2 * R, R), 2 * R)
     load(cos_ref.at[table], cosb)
     load(sin_ref.at[table], sinb)
-
-    barrier = pltpu.get_barrier_semaphore()
-    for peer in (X, Y, PAIR):
-        pl.semaphore_signal(barrier, inc=1, device_id=peer, device_id_type=MESH)
-
-    @pl.when(z < chips - 1)
-    def _():
-        pl.semaphore_signal(barrier, inc=1, device_id={"sp": sp, "dp": dp + 2}, device_id_type=MESH)
-
-    @pl.when(z > 0)
-    def _():
-        pl.semaphore_signal(barrier, inc=1, device_id={"sp": sp, "dp": dp - 2}, device_id_type=MESH)
+    for source, target in ((ig_in, ig_ref), (qg_in, qg_ref), (kg_in, kg_ref), (og_in, og_ref)):
+        load(source, target)
 
     in_chain = (z + others) // chips + (2 * others - z) // chips
     pl.semaphore_wait(barrier, 3 + in_chain)
 
-    pending = []
-
-    def send(ref, sems, recvs, index, peer, dst=None):
-        copy = remote(ref, ref if dst is None else dst, sems.at[index], recvs.at[index], peer)
-        copy.start()
-        pending.append(copy)
+    def send(make, sems, recvs, index, peer, make_dst=None):
+        slot = index[0] if isinstance(index, tuple) else 0
+        for src, dst in zip(make(), (make_dst or make)()):
+            remote(src, dst, sems.at[slot], recvs.at[index], peer).start()
+
+    def sent(ref, sems, slot):
+        remote(ref, ref, sems.at[slot], p_recv.at[0], PAIR).wait_send()
 
     def arrived(ref, recvs, index):
-        remote(ref, ref, p_send.at[0, 0], recvs.at[index], PAIR).wait_recv()
+        remote(ref, ref, p_send.at[0], recvs.at[index], PAIR).wait_recv()
 
     def rows(owner, of, start=0, size=depth):
         return pl.ds(pl.multiple_of((owner * 2 + of) * depth, depth) + start, size)
 
-    def quarter(owner, of, who, start=0, size=depth):
-        return wob.at[rows(owner, of, start, size), pl.ds(pl.multiple_of(who * share, 128), share)]
+    def quarter(owner, of, who, a=0, b=2):
+        broad = wob.at[rows(owner, of, a * depth // 2, (b - a) * depth // 2),
+                       pl.ds(pl.multiple_of(who * wide, 128), wide)]
+        slim = wob.at[rows(owner, of, a * shared // 2, (b - a) * shared // 2),
+                      pl.ds(pl.multiple_of(4 * wide + who * narrow, 128), narrow)]
+        return [broad, slim]
+
+    def quarters(times, a=0, b=2):
+        return wob.at[:times * (b - a) * (depth // 2 + shared // 4), :wide]
+
+    def rests(times):
+        return wob.at[:times * (2 * depth - shared), :rest]
 
     def block(t, owner, of, j=None):
         if t == 0:
-            return wkv.at[yi if j is None else j, rows(owner, of)]
+            return [wkv.at[yi if j is None else j, rows(owner, of)]]
         if t == 1:
-            return wqb.at[yi if j is None else j, rows(owner, of)]
+            return [wqb.at[yi if j is None else j, rows(owner, of)]]
         if t == 2:
             return quarter(owner, of, sp)
-        return wob.at[rows(owner, of), pl.ds(4 * share, rest)]
+        return [wob.at[rows(owner, of), pl.ds(OD - rest, rest)],
+                wob.at[rows(owner, of, shared, depth - shared), pl.ds(4 * wide, 4 * narrow)]]
+
+    def bulk(t):
+        if t == 0:
+            return wkv.at[0, :depth]
+        if t == 1:
+            return wqb.at[0, :depth]
+        return quarters(1) if t == 2 else rests(1)
 
     low = jnp.minimum(z, others - z)
 
@@ -510,13 +531,22 @@
 
         @pl.when(ok)
         def _():
-            ref = block(t, z, core)
-            remote(ref, ref, z_own.at[t, int(up)], z_recv.at[t, z],
-                   {"sp": sp, "dp": dp + (2 if up else -2)}).start()
-
-    def to_pair(kind, owner, ref):
-        remote(ref, ref, p_send.at[kind, owner], p_recv.at[kind, owner], PAIR).start()
-        pending.append(remote(ref, ref, p_send.at[kind, owner], p_recv.at[kind, owner], PAIR))
+            for ref in block(t, z, core):
+                remote(ref, ref, z_own.at[t, int(up)], z_recv.at[t, z],
+                       {"sp": sp, "dp": dp + (2 if up else -2)}).start()
+
+    def to_pair(kind, refs):
+        group = {0: 0, 4: 0, 1: 1, 5: 2, 2: 3, 7: 4, 6: 5, 8: 6, 9: 6, 3: 7}[kind]
+        for ref in refs:
+            remote(ref, ref, p_send.at[group], p_recv.at[group], PAIR).start()
+
+    def pair_refs():
+        half = wqb.at[0, :F // 2]
+        return [wkv.at[0], half, half] + [quarters(others)] * 4 + [rests(others)]
+
+    def pair_wait(group):
+        ref = pair_refs()[group]
+        remote(ref, ref, p_send.at[group], p_recv.at[group], PAIR).wait_recv()
 
     def relay_target(owner):
         step = jnp.where(owner < z, 1, -1)
@@ -524,66 +554,68 @@
 
     def from_z(t, i):
         owner = owners[i]
-        ref = block(t, owner, core)
-        arrived(ref, z_recv, (t, owner))
+        arrived(bulk(t), z_recv, (t, owner))
         ok, peer = relay_target(owner)
 
         @pl.when(ok)
         def _():
-            remote(ref, ref, z_send.at[t, owner], z_recv.at[t, owner], peer).start()
-
-        if t < 3:
-            send(ref, y_send, y_recv, (t, owner), Y)
+            for ref in block(t, owner, core):
+                remote(ref, ref, z_send.at[t, owner], z_recv.at[t, owner], peer).start()
+
+        def make():
+            return block(t, owner, core)
+
+        if t < 2:
+            send(make, y_send, y_recv, (t, owner), Y)
         if t == 2:
-            send(ref, x_send, x_recv, (0, owner), X)
-        to_pair(t, owner, ref)
+            send(make, x_send, x_recv, (0, owner), X)
+        to_pair(t, make())
+
+    def share_y(i):
+        owner = owners[i]
+        send(lambda: block(2, owner, core), y_send, y_recv, (2, owner), Y)
 
     def from_y(t, i):
         owner = owners[i]
-        if t < 2:
-            ref = block(t, owner, core, 1 - yi)
+        arrived(bulk(t), y_recv, (t, owner))
+        if t == 2:
+            send(lambda: quarter(owner, core, y_peer, 0, 1), x_send, x_recv, (1, owner), X)
+            to_pair(6, quarter(owner, core, y_peer))
         else:
-            ref = quarter(owner, core, y_peer)
-        arrived(ref, y_recv, (t, owner))
-        if t == 2:
-            send(quarter(owner, core, y_peer, 0, half), x_send, x_recv, (1, owner), X)
-        to_pair(4 + t, owner, ref)
+            to_pair(4 + t, block(t, owner, core, 1 - yi))
 
     def from_x(i):
         owner = owners[i]
-        ref = quarter(owner, core, x_peer)
-        arrived(ref, x_recv, (0, owner))
-        send(quarter(owner, core, x_peer, half, half), y_send, y_recv, (3, owner), Y)
-        to_pair(7, owner, ref)
-
-    def from_corner(i):
+        arrived(bulk(2), x_recv, (0, owner))
+        send(lambda: quarter(owner, core, x_peer, 1, 2), y_send, y_recv, (3, owner), Y)
+        to_pair(7, quarter(owner, core, x_peer))
+
+    def corner_x(i):
         owner = owners[i]
-        ref = quarter(owner, core, corner, 0, half)
-        arrived(ref, x_recv, (1, owner))
-        to_pair(8, owner, ref)
-        ref = quarter(owner, core, corner, half, half)
-        arrived(ref, y_recv, (3, owner))
-        to_pair(9, owner, ref)
-
-    def pair_has(kind, ref, owner):
-        arrived(ref, p_recv, (kind, owner))
-
-    send(x_ref, tok_send, tok_recv, 0, X, xn.at[pl.ds(pl.multiple_of(xi * R, R), R)])
-    for copy in loads[:4]:
+        arrived(quarters(1, 0, 1), x_recv, (1, owner))
+        to_pair(8, quarter(owner, core, corner, 0, 1))
+
+    def corner_y(i):
+        owner = owners[i]
+        arrived(quarters(1, 1, 2), y_recv, (3, owner))
+        to_pair(9, quarter(owner, core, corner, 1, 2))
+
+    for copy in loads[:5]:
         copy.wait()
+    send(lambda: [x_ref], tok_send, tok_recv, 0, X, lambda: [xn.at[pl.ds(pl.multiple_of(xi * R, R), R)]])
     start_own(0, True)
     start_own(0, False)
-    to_pair(0, z, block(0, z, core))
-    to_pair(4, z, block(0, z, core, 1 - yi))
-    for copy in loads[4:6]:
+    to_pair(0, block(0, z, core))
+    to_pair(4, block(0, z, core, 1 - yi))
+    for copy in loads[5:7]:
         copy.wait()
     start_own(1, True)
     start_own(1, False)
-    to_pair(1, z, block(1, z, core))
-    to_pair(5, z, block(1, z, core, 1 - yi))
-    for copy in loads[6:]:
+    to_pair(1, block(1, z, core))
+    to_pair(5, block(1, z, core, 1 - yi))
+    for copy in loads[7:]:
         copy.wait()
-    to_pair(2, z, wob.at[mine])
+    remote(wob.at[mine], wob.at[mine], own_send.at[0], own_recv.at[0], PAIR).start()
 
     def normalize(values, start):
         x = values.astype(jnp.float32)
@@ -594,16 +626,37 @@
         start_own(t, True, now)
         start_own(t, False, now)
 
+    inner = low > 0
+
+    def quarter_stage(i, early):
+        @pl.when(inner if early else jnp.logical_not(inner))
+        def _():
+            from_z(2, i)
+            stage_own(3, i)
+
+    def rest_stage(i, early):
+        @pl.when(inner if early else jnp.logical_not(inner))
+        def _():
+            from_z(3, i)
+
+    def quarter_late(i):
+        quarter_stage(i, False)
+        share_y(i)
+
     normalize(x_ref[...], xi * R)
     stage_own(2, 0)
+    stage_own(3, 0)
     for i in range(1, chips):
         from_z(0, i)
+        if i > 2:
+            from_y(1, i - 2)
         if i > 1:
-            from_y(1, i - 1)
+            from_y(0, i - 1)
         from_z(1, i)
         stage_own(2, i)
-        from_y(0, i)
-
+
+    for i in range(1, chips):
+        quarter_stage(i, True)
     lane = lax.broadcasted_iota(jnp.int32, (R, HEAD_WIDTH), 1)
     first = lane % (HEAD_WIDTH // 2) < HEAD_WIDTH // 4
 
@@ -616,11 +669,12 @@
     def cut(values, h):
         return values[:, h * HEAD_WIDTH:(h + 1) * HEAD_WIDTH]
 
-    for owner in range(chips):
-        pair_has(0, block(0, owner, 1 - core), owner)
-        pair_has(4, block(0, owner, 1 - core, 1 - yi), owner)
-
-    def keys_values(who):
+    if chips > 2:
+        from_y(1, others - 1)
+    from_y(0, others)
+    pair_wait(0)
+
+    def keys_values(turn, who):
         local = pl.ds(pl.multiple_of(who * R, R), R)
         placed = pl.ds(pl.multiple_of((yi * 2 + who) * R, R), R)
         cosine, sine = cosb[local], sinb[local]
@@ -631,13 +685,14 @@
                 kv_buf[placed, start:start + HEAD_WIDTH] = finish(cut(mixed, h), kg_ref[...], cosine, sine)
             start = 2 * kv_width + j * kv_width
             kv_buf[placed, start:start + kv_width] = mixed[:, kv_width:].astype(jnp.bfloat16)
-        return kv_buf.at[placed]
-
-    send(keys_values(xi), kv_send, kv_recv, 0, Y)
+        send(lambda: [kv_buf.at[pl.ds(pl.multiple_of((yi * 2 + who) * R, R), R)]],
+             kv_send, kv_recv, turn, Y)
+
+    keys_values(0, xi)
     theirs = xn.at[pl.ds(pl.multiple_of((1 - xi) * R, R), R)]
     arrived(theirs, tok_recv, 0)
     normalize(theirs[...], (1 - xi) * R)
-    send(keys_values(1 - xi), kv_send, kv_recv, 1, Y)
+    keys_values(1, 1 - xi)
 
     def queries(j):
         @pl.loop(0, 2)
@@ -649,20 +704,19 @@
                 at = pl.ds(pl.multiple_of(j * q_width + h * HEAD_WIDTH, HEAD_WIDTH), HEAD_WIDTH)
                 q_buf[local, at] = finish(cut(mixed, h), qg_ref[...], cosine, sine)
 
-    stage_own(3, 0)
-    from_z(2, 1)
-    stage_own(3, 1)
-    for owner in range(chips):
-        pair_has(1, block(1, owner, 1 - core), owner)
+    quarter_late(1)
+    pair_wait(1)
     queries(yi)
+    for i in range(min(2, others), 0, -1):
+        rest_stage(i, True)
+    from_y(1, others)
+    pair_wait(2)
+    queries(1 - yi)
     for i in range(2, chips):
-        from_z(2, i)
-        stage_own(3, i)
-    from_y(1, others)
-    for owner in range(chips):
-        pair_has(5, block(1, owner, 1 - core, 1 - yi), owner)
-    queries(1 - yi)
+        quarter_late(i)
     from_x(1)
+    for i in range(3, chips):
+        rest_stage(i, True)
     for who in range(2):
         at = pl.ds(pl.multiple_of(((1 - yi) * 2 + (who + xi) % 2) * R, R), R)
         arrived(kv_buf.at[at], kv_recv, who)
@@ -673,9 +727,10 @@
 
     def attend(step):
         turn = step % steps
-        who = jnp.where(step < steps, 1 - xi, xi)
+        who = 1 - xi if step < steps else xi
         local = pl.ds(pl.multiple_of(who * R, R), R)
-        base = jnp.where(step < steps, 2 * width, xi * width) + turn * couple * HEAD_WIDTH
+        place = 2 if step < steps else xi
+        base = turn * couple * HEAD_WIDTH
         for u in range(couple):
             head = turn * couple + u
             group = head // (per // kv_per)
@@ -687,14 +742,13 @@
             top = jnp.max(scores, axis=-1, keepdims=True)
             raised = jnp.exp2((scores - top) * factor)
             weights = (raised * (1.0 / jnp.sum(raised, axis=-1, keepdims=True))).astype(jnp.bfloat16)
-            att[:, pl.ds(pl.multiple_of(base + u * HEAD_WIDTH, HEAD_WIDTH), HEAD_WIDTH)] = jnp.dot(
+            att[place, :, base + u * HEAD_WIDTH:base + (u + 1) * HEAD_WIDTH] = jnp.dot(
                 weights, kv_buf[:, v_at], preferred_element_type=jnp.float32).astype(jnp.bfloat16)
 
     def give(turn):
         size = couple * HEAD_WIDTH
-        src = att.at[:, pl.ds(2 * width + turn * size, size)]
-        dst = att.at[:, pl.ds(pl.multiple_of(xi * width + turn * size, 128), size)]
-        send(src, att_send, att_recv, turn, X, dst)
+        send(lambda: [att.at[2, :, pl.ds(turn * size, size)]], att_send, att_recv, 0, X,
+             lambda: [att.at[xi, :, pl.ds(turn * size, size)]])
 
     last = 2 * steps - 1
     timed = []
@@ -702,8 +756,7 @@
         if i > 1:
             timed.append((2 * i - 3, lambda i=i: from_x(i)))
         timed.append((3 * i - 1, lambda i=i: from_y(2, i)))
-        timed.append((2 * i + 1, lambda i=i: from_z(3, i)))
-        timed.append((last, lambda i=i: from_corner(i)))
+        timed.append((3 * i - 1, lambda i=i: rest_stage(i, False)))
     work = [[item for when, item in timed if min(when, last) == step] for step in range(2 * steps)]
 
     for step in range(2 * steps):
@@ -713,44 +766,67 @@
         for item in work[step]:
             item()
 
-    for turn in range(steps):
-        size = couple * HEAD_WIDTH
-        ref = att.at[:, pl.ds(pl.multiple_of((1 - xi) * width + turn * size, 128), size)]
-        arrived(ref, att_recv, turn)
-    for i in range(chips):
-        owner = owners[i]
-        if i == 0:
-            pair_has(2, wob.at[rows(owner, 1 - core)], owner)
-        else:
-            pair_has(2, quarter(owner, 1 - core, sp), owner)
-            pair_has(6, quarter(owner, 1 - core, y_peer), owner)
-            pair_has(7, quarter(owner, 1 - core, x_peer), owner)
-            pair_has(8, quarter(owner, 1 - core, corner, 0, half), owner)
-            pair_has(9, quarter(owner, 1 - core, corner, half, half), owner)
-            pair_has(3, block(3, owner, 1 - core), owner)
-
-    tile = OD // 4
-
-    @pl.loop(0, 4)
-    def _(n):
-        at = pl.ds(pl.multiple_of(n * tile, 128), tile)
-        total[:, at] = jnp.dot(att[:, :2 * width], wob[:, at], preferred_element_type=jnp.float32)
-
-    x = total[...]
-    scale = lax.rsqrt(jnp.mean(x * x, axis=-1, keepdims=True) + EPS)
-    o_ref[...] = (x * scale * og_ref[...]).astype(jnp.bfloat16)
-
-    for copy in pending:
-        copy.wait_send()
+    def project(zones, mine):
+        half = xi if mine else 1 - xi
+        left = att[half]
+        deep = pl.ds(pl.multiple_of(half * width, width), width)
+        for at in zones:
+            part = jnp.dot(left, wob[deep, at], preferred_element_type=jnp.float32)
+            total[:, at] = part if mine else total[:, at] + part
+
+    def zone(who):
+        return pl.ds(pl.multiple_of(who * wide, 128), wide)
+
+    arrived(wob.at[rows(z, 1 - core)], own_recv, 0)
+    pair_wait(3)
+    pair_wait(4)
+    project([zone(sp), zone(x_peer)], True)
+    pair_wait(5)
+    pair_wait(7)
+    project([zone(y_peer), pl.ds(OD - rest, rest)], True)
+    for i in range(1, chips):
+        corner_y(i)
+        corner_x(i)
+    arrived(att.at[1 - xi], att_recv, 0)
+    project([pl.ds(OD - rest, rest), zone(sp), zone(x_peer), zone(y_peer)], False)
+    pair_wait(6)
+    late = [zone(corner), pl.ds(4 * wide, 4 * narrow)]
+    project(late, True)
+    project(late, False)
+
+    chunk = R // 4
+    stores = []
+    for n in range(4):
+        at = pl.ds(n * chunk, chunk)
+        x = total[at]
+        scale = lax.rsqrt(jnp.mean(x * x, axis=-1, keepdims=True) + EPS)
+        out[at] = (x * scale * og_ref[...]).astype(jnp.bfloat16)
+        store = pltpu.make_async_copy(out.at[at], o_ref.at[at], load_sem.at[n])
+        store.start()
+        stores.append(store)
+
+    count = others * depth
+    sent(x_ref, tok_send, 0)
+    sent(wkv.at[0, :count], y_send, 0)
+    sent(wqb.at[0, :count], y_send, 1)
+    sent(quarters(others), y_send, 2)
+    sent(quarters(others, 1, 2), y_send, 3)
+    sent(quarters(others), x_send, 0)
+    sent(quarters(others, 0, 1), x_send, 1)
+    sent(kv_buf.at[:2 * R], kv_send, 0)
+    sent(att.at[2], att_send, 0)
+    for group, ref in enumerate(pair_refs()):
+        sent(ref, p_send, group)
+    sent(wob.at[mine], own_send, 0)
     for t in range(4):
         @pl.when(z < others)
         def _():
-            ref = block(t, z, core)
+            ref = bulk(t)
             remote(ref, ref, z_own.at[t, 1], z_recv.at[t, z], PAIR).wait_send()
 
         @pl.when(z > 0)
         def _():
-            ref = block(t, z, core)
+            ref = bulk(t)
             remote(ref, ref, z_own.at[t, 0], z_recv.at[t, z], PAIR).wait_send()
 
         for i in range(1, chips):
@@ -759,8 +835,11 @@
 
             @pl.when(ok)
             def _():
-                ref = block(t, owner, core)
+                ref = bulk(t)
                 remote(ref, ref, z_send.at[t, owner], z_recv.at[t, owner], peer).wait_send()
+
+    for store in stores:
+        store.wait()
 
 
 def fused(sequence, in_gain, query_weight, key_weight, value_matrix, query_gain, key_gain,
@@ -769,29 +848,32 @@
     q_width, kv_width = query_weight.shape[1] // 4, key_weight.shape[1] // 4
     columns = out_weight.shape[1]
     dma = pltpu.SemaphoreType.DMA
-    vmem = pl.BlockSpec(memory_space=pltpu.VMEM)
     bf16, f32 = jnp.bfloat16, jnp.float32
-    steps = q_width // HEAD_WIDTH
     return pl.pallas_call(
         functools.partial(fused_kernel, chips, q_width, kv_width),
         out_shape=jax.ShapeDtypeStruct((row_count, columns), bf16),
-        in_specs=[vmem, ANY, ANY, ANY, ANY, vmem, vmem, vmem, ANY, ANY, vmem],
-        out_specs=vmem,
+        in_specs=[ANY] * 11,
+        out_specs=ANY,
         scratch_shapes=[
+            pltpu.VMEM((row_count, features), bf16),
+            pltpu.VMEM((1, features), f32),
+            pltpu.VMEM((1, HEAD_WIDTH), f32),
+            pltpu.VMEM((1, HEAD_WIDTH), f32),
+            pltpu.VMEM((1, columns), f32),
             pltpu.VMEM((2 * row_count, features), bf16),
             pltpu.VMEM((2, features, 2 * kv_width), bf16),
             pltpu.VMEM((2, features, q_width), bf16),
             pltpu.VMEM((out_weight.shape[0] * chips * 2, columns), bf16),
             pltpu.VMEM((2 * row_count, 2 * q_width), bf16),
             pltpu.VMEM((4 * row_count, 4 * kv_width), bf16),
-            pltpu.VMEM((row_count, 6 * q_width), bf16),
+            pltpu.VMEM((3, row_count, 2 * q_width), bf16),
             pltpu.VMEM((row_count, columns), f32),
+            pltpu.VMEM((row_count, columns), bf16),
             pltpu.VMEM((2 * row_count, HEAD_WIDTH), f32),
             pltpu.VMEM((2 * row_count, HEAD_WIDTH), f32),
-            dma((9,)), dma((1,)), dma((1,)), dma((4, 2)), dma((4, chips)), dma((4, chips)),
-            dma((4, chips)), dma((4, chips)), dma((2, chips)), dma((2, chips)),
-            dma((2,)), dma((2,)), dma((steps,)), dma((steps,)),
-            dma((10, chips)), dma((10, chips)),
+            dma((14,)), dma((1,)), dma((1,)), dma((4, 2)), dma((4, chips)), dma((4, chips)),
+            dma((4,)), dma((4, chips)), dma((2,)), dma((2, chips)),
+            dma((1,)), dma((2,)), dma((1,)), dma((1,)), dma((8,)), dma((8,)), dma((1,)), dma((1,)),
         ],
         compiler_params=pltpu.CompilerParams(
             collective_id=0, has_side_effects=True, vmem_limit_bytes=60 * 1024 * 1024),

time: 88.5 us -> 77 us (0.87)
  Pallas kernels: 86 us -> 74.3 us
    pallas_call x1, Pallas kernels: 86 us -> 74.3 us  [fused(): pl.pallas_call(functools.partial(fused_kernel, chips, q_width, kv_width),...]
where the time goes in v2:
time: 77 us; the launch traced here: 76.6 us
  Pallas kernels  74.3 us (96%)
  local copies, waits for them, and re-layouts  2.3 us (3%)
    pallas_call x1, Pallas kernels, fused(): pl.pallas_call(functools.partial(fused_kernel, chips, q_width, kv_width),...  74.3 us
    unnamed x1, local copies, waits for them, and re-layouts  2.3 us

profile of v2, /device:TPU:1, one launch (start us, length us, event | category | flops | bytes accessed | tf_op | source)
XLA Modules:
  0.0 76.6 jit_solution(12994721371969821441)
XLA Ops:
  0.0 74.3 %attention_layer.1 = bf16[256,2048]{1,0:T(8,128)(2,1)} custom-call(bf16[256,2048]{1,0:T(8,128)(2,1)} %bitcast.7, bf16[256,2048]{1,0:T(8,128)(2,1)} %wq_ref.1, bf16[256,512]{1,0:T(8,128)(2,1)} %wk_ref.1, bf16[256,512]{1,0:T(8,128)(2,1)} %wv_ref.1, bf16[256,2048]{1,0:T(8,128)(2,1)} %wo_ref.1, f32[1,2048]{1,0:T(1,128)} %bitcast.8, f32[1,128]{1,0:T(1,128)} %bitcast.10, ...), custom_call_target="tpu_custom_call" | custom-call | flops 10000000000 | bytes 10000000 | tf_op jit(solution)/shard_map/attention_layer/pallas_call | solution.py:852
  74.3 2.3 %copy.13 = bf16[1,256,2048]{2,1,0:T(8,128)(2,1)} copy(bf16[1,256,2048]{2,1,0:T(8,128)(2,1)} %bitcast.6) | data formatting | bytes 2097152

commit v3 on v2

--- a/solution.py
+++ b/solution.py
@@ -405,9 +405,9 @@
 
 def fused_kernel(
     chips, q_width, kv_width,
-    x_in, wq_ref, wk_ref, wv_ref, wo_ref, ig_in, qg_in, kg_in, cos_ref, sin_ref, og_in,
-    o_ref,
-    x_ref, ig_ref, qg_ref, kg_ref, og_ref, xn, wkv, wqb, wob, q_buf, kv_buf, att, total, out, cosb, sinb,
+    x_in, wq_ref, wk_ref, wv_ref, wo_ref, ig_in, qg_in, kg_in, cos_ref, sin_ref,
+    total,
+    x_ref, ig_ref, qg_ref, kg_ref, xn, wkv, wqb, wob, q_buf, kv_buf, att, cosb, sinb,
     load_sem, tok_send, tok_recv, z_own, z_send, z_recv, y_send, y_recv, x_send, x_recv,
     kv_send, kv_recv, att_send, att_recv, p_send, p_recv, own_send, own_recv,
 ):
@@ -461,7 +461,7 @@
     table = pl.ds(pl.multiple_of(yi * 2 * R, R), 2 * R)
     load(cos_ref.at[table], cosb)
     load(sin_ref.at[table], sinb)
-    for source, target in ((ig_in, ig_ref), (qg_in, qg_ref), (kg_in, kg_ref), (og_in, og_ref)):
+    for source, target in ((ig_in, ig_ref), (qg_in, qg_ref), (kg_in, kg_ref)):
         load(source, target)
 
     in_chain = (z + others) // chips + (2 * others - z) // chips
@@ -524,6 +524,17 @@
     above = others - z
     last_above = jnp.where(above == 0, 0, jnp.where(above <= z, 2 * above, others))
 
+    def start_q(up, part, when=None):
+        ok = z < others if up else z > 0
+        if when is not None:
+            ok = jnp.logical_and(ok, when)
+
+        @pl.when(ok)
+        def _():
+            ref = wqb.at[yi, rows(z, core, part * (depth // 2), depth // 2)]
+            remote(ref, ref, z_own.at[1, int(up)], z_recv.at[1, z],
+                   {"sp": sp, "dp": dp + (2 if up else -2)}).start()
+
     def start_own(t, up, now=None):
         ok = z < others if up else z > 0
         if now is not None:
@@ -536,13 +547,14 @@
                        {"sp": sp, "dp": dp + (2 if up else -2)}).start()
 
     def to_pair(kind, refs):
-        group = {0: 0, 4: 0, 1: 1, 5: 2, 2: 3, 7: 4, 6: 5, 8: 6, 9: 6, 3: 7}[kind]
+        group = {0: 0, 4: 0, 1: 1, 5: 2, 2: 3, 7: 4, 6: 5, 8: 6, 9: 6, 3: 7, 10: 8, 11: 9}[kind]
         for ref in refs:
             remote(ref, ref, p_send.at[group], p_recv.at[group], PAIR).start()
 
     def pair_refs():
         half = wqb.at[0, :F // 2]
-        return [wkv.at[0], half, half] + [quarters(others)] * 4 + [rests(others)]
+        return ([wkv.at[0], half, half] + [quarters(others)] * 3
+                + [quarters(others - 1), rests(others - 1), rests(1), quarters(1)])
 
     def pair_wait(group):
         ref = pair_refs()[group]
@@ -565,15 +577,15 @@
         def make():
             return block(t, owner, core)
 
-        if t < 2:
+        if t == 0 or (t == 1 and i < others):
             send(make, y_send, y_recv, (t, owner), Y)
         if t == 2:
             send(make, x_send, x_recv, (0, owner), X)
-        to_pair(t, make())
-
-    def share_y(i):
+        to_pair(10 if t == 3 and i == others else t, make())
+
+    def share_y(t, i):
         owner = owners[i]
-        send(lambda: block(2, owner, core), y_send, y_recv, (2, owner), Y)
+        send(lambda: block(t, owner, core), y_send, y_recv, (t, owner), Y)
 
     def from_y(t, i):
         owner = owners[i]
@@ -593,12 +605,12 @@
     def corner_x(i):
         owner = owners[i]
         arrived(quarters(1, 0, 1), x_recv, (1, owner))
-        to_pair(8, quarter(owner, core, corner, 0, 1))
+        to_pair(11 if i == others else 8, quarter(owner, core, corner, 0, 1))
 
     def corner_y(i):
         owner = owners[i]
         arrived(quarters(1, 1, 2), y_recv, (3, owner))
-        to_pair(9, quarter(owner, core, corner, 1, 2))
+        to_pair(11 if i == others else 9, quarter(owner, core, corner, 1, 2))
 
     for copy in loads[:5]:
         copy.wait()
@@ -609,8 +621,8 @@
     to_pair(4, block(0, z, core, 1 - yi))
     for copy in loads[5:7]:
         copy.wait()
-    start_own(1, True)
-    start_own(1, False)
+    start_q(True, 0)
+    start_q(False, 0)
     to_pair(1, block(1, z, core))
     to_pair(5, block(1, z, core, 1 - yi))
     for copy in loads[7:]:
@@ -627,36 +639,39 @@
         start_own(t, False, now)
 
     inner = low > 0
-
-    def quarter_stage(i, early):
-        @pl.when(inner if early else jnp.logical_not(inner))
+    outer = jnp.logical_not(inner)
+
+    def only(when, *stages):
+        @pl.when(when)
         def _():
-            from_z(2, i)
-            stage_own(3, i)
-
-    def rest_stage(i, early):
-        @pl.when(inner if early else jnp.logical_not(inner))
-        def _():
-            from_z(3, i)
-
-    def quarter_late(i):
-        quarter_stage(i, False)
-        share_y(i)
+            for stage in stages:
+                stage()
+
+    def columns_in(i):
+        from_z(1, i)
+        stage_own(2, i)
+
+    def quarter_in(i):
+        from_z(2, i)
+        stage_own(3, i)
 
     normalize(x_ref[...], xi * R)
-    stage_own(2, 0)
-    stage_own(3, 0)
     for i in range(1, chips):
         from_z(0, i)
+        if i == 1:
+            start_q(True, 1)
+            start_q(False, 1, outer)
+            stage_own(2, 0)
+            stage_own(3, 0)
+        if i == min(2, others):
+            start_q(False, 1, inner)
+        if i > 1:
+            from_y(0, i - 1)
+            columns_in(i - 1)
         if i > 2:
             from_y(1, i - 2)
-        if i > 1:
-            from_y(0, i - 1)
-        from_z(1, i)
-        stage_own(2, i)
-
-    for i in range(1, chips):
-        quarter_stage(i, True)
+    only(inner, lambda: columns_in(others), *[functools.partial(quarter_in, i) for i in range(1, others)])
+
     lane = lax.broadcasted_iota(jnp.int32, (R, HEAD_WIDTH), 1)
     first = lane % (HEAD_WIDTH // 2) < HEAD_WIDTH // 4
 
@@ -669,9 +684,8 @@
     def cut(values, h):
         return values[:, h * HEAD_WIDTH:(h + 1) * HEAD_WIDTH]
 
-    if chips > 2:
-        from_y(1, others - 1)
-    from_y(0, others)
+    if chips > 1:
+        from_y(0, others)
     pair_wait(0)
 
     def keys_values(turn, who):
@@ -681,14 +695,14 @@
         for j in range(2):
             mixed = jnp.dot(xn[local], wkv[j], preferred_element_type=jnp.float32)
             for h in range(kv_per):
-                start = j * kv_width + h * HEAD_WIDTH
-                kv_buf[placed, start:start + HEAD_WIDTH] = finish(cut(mixed, h), kg_ref[...], cosine, sine)
-            start = 2 * kv_width + j * kv_width
-            kv_buf[placed, start:start + kv_width] = mixed[:, kv_width:].astype(jnp.bfloat16)
-        send(lambda: [kv_buf.at[pl.ds(pl.multiple_of((yi * 2 + who) * R, R), R)]],
+                kv_buf[j, placed, h * HEAD_WIDTH:(h + 1) * HEAD_WIDTH] = finish(
+                    cut(mixed, h), kg_ref[...], cosine, sine)
+            kv_buf[j, placed, kv_width:] = mixed[:, kv_width:].astype(jnp.bfloat16)
+        send(lambda: [kv_buf.at[:, pl.ds(pl.multiple_of((yi * 2 + who) * R, R), R)]],
              kv_send, kv_recv, turn, Y)
 
     keys_values(0, xi)
+    only(outer, lambda: columns_in(others))
     theirs = xn.at[pl.ds(pl.multiple_of((1 - xi) * R, R), R)]
     arrived(theirs, tok_recv, 0)
     normalize(theirs[...], (1 - xi) * R)
@@ -701,109 +715,125 @@
             cosine, sine = cosb[local], sinb[local]
             mixed = jnp.dot(xn[local], wqb[j], preferred_element_type=jnp.float32)
             for h in range(per):
-                at = pl.ds(pl.multiple_of(j * q_width + h * HEAD_WIDTH, HEAD_WIDTH), HEAD_WIDTH)
-                q_buf[local, at] = finish(cut(mixed, h), qg_ref[...], cosine, sine)
-
-    quarter_late(1)
+                q_buf[j, local, h * HEAD_WIDTH:(h + 1) * HEAD_WIDTH] = finish(
+                    cut(mixed, h), qg_ref[...], cosine, sine)
+
+    share_y(1, others)
+    only(inner, lambda: quarter_in(others))
+    if chips > 2:
+        from_y(1, others - 1)
+    only(outer, lambda: quarter_in(1))
+    share_y(2, 1)
     pair_wait(1)
     queries(yi)
     for i in range(min(2, others), 0, -1):
-        rest_stage(i, True)
-    from_y(1, others)
-    pair_wait(2)
-    queries(1 - yi)
+        only(inner, lambda i=i: from_z(3, i))
     for i in range(2, chips):
-        quarter_late(i)
+        only(outer, lambda i=i: quarter_in(i))
+        share_y(2, i)
     from_x(1)
-    for i in range(3, chips):
-        rest_stage(i, True)
     for who in range(2):
         at = pl.ds(pl.multiple_of(((1 - yi) * 2 + (who + xi) % 2) * R, R), R)
-        arrived(kv_buf.at[at], kv_recv, who)
+        arrived(kv_buf.at[:, at], kv_recv, who)
 
     factor = HEAD_WIDTH ** (-0.5) * float(np.log2(np.e))
     couple = 2
-    steps = 2 * per // couple
-
-    def attend(step):
-        turn = step % steps
-        who = 1 - xi if step < steps else xi
+    turns = per // couple
+
+    def attend(mine, j, turn):
+        who, place = (xi, xi) if mine else (1 - xi, 2)
         local = pl.ds(pl.multiple_of(who * R, R), R)
-        place = 2 if step < steps else xi
-        base = turn * couple * HEAD_WIDTH
         for u in range(couple):
             head = turn * couple + u
-            group = head // (per // kv_per)
-            k_at = pl.ds(pl.multiple_of(group * HEAD_WIDTH, HEAD_WIDTH), HEAD_WIDTH)
-            v_at = pl.ds(pl.multiple_of(2 * kv_width + group * HEAD_WIDTH, HEAD_WIDTH), HEAD_WIDTH)
-            q_at = pl.ds(pl.multiple_of(head * HEAD_WIDTH, HEAD_WIDTH), HEAD_WIDTH)
-            scores = lax.dot_general(q_buf[local, q_at], kv_buf[:, k_at], (((1,), (1,)), ((), ())),
-                                     preferred_element_type=jnp.float32)
+            group = head // (per // kv_per) * HEAD_WIDTH
+            at = slice(head * HEAD_WIDTH, (head + 1) * HEAD_WIDTH)
+            scores = lax.dot_general(
+                q_buf[j, local, at], kv_buf[j, :, group:group + HEAD_WIDTH], (((1,), (1,)), ((), ())),
+                preferred_element_type=jnp.float32)
             top = jnp.max(scores, axis=-1, keepdims=True)
             raised = jnp.exp2((scores - top) * factor)
             weights = (raised * (1.0 / jnp.sum(raised, axis=-1, keepdims=True))).astype(jnp.bfloat16)
-            att[place, :, base + u * HEAD_WIDTH:base + (u + 1) * HEAD_WIDTH] = jnp.dot(
-                weights, kv_buf[:, v_at], preferred_element_type=jnp.float32).astype(jnp.bfloat16)
-
-    def give(turn):
-        size = couple * HEAD_WIDTH
-        send(lambda: [att.at[2, :, pl.ds(turn * size, size)]], att_send, att_recv, 0, X,
-             lambda: [att.at[xi, :, pl.ds(turn * size, size)]])
-
-    last = 2 * steps - 1
-    timed = []
+            values = kv_buf[j, :, kv_width + group:kv_width + group + HEAD_WIDTH]
+            att[place, j, :, at] = jnp.dot(
+                weights, values, preferred_element_type=jnp.float32).astype(jnp.bfloat16)
+
+    def give(j, turn):
+        at = pl.ds(turn * couple * HEAD_WIDTH, couple * HEAD_WIDTH)
+        send(lambda: [att.at[2, j, :, at]], att_send, att_recv, 0, X, lambda: [att.at[xi, j, :, at]])
+
+    early, late = [], []
+    for i in range(2, others):
+        early.append(lambda i=i: from_x(i))
+    for i in range(max(2, others), chips):
+        late.append(lambda i=i: from_x(i))
     for i in range(1, chips):
         if i > 1:
-            timed.append((2 * i - 3, lambda i=i: from_x(i)))
-        timed.append((3 * i - 1, lambda i=i: from_y(2, i)))
-        timed.append((3 * i - 1, lambda i=i: rest_stage(i, False)))
-    work = [[item for when, item in timed if min(when, last) == step] for step in range(2 * steps)]
-
-    for step in range(2 * steps):
-        attend(step)
-        if step < steps:
-            give(step)
-        for item in work[step]:
-            item()
+            late.append(lambda i=i: from_y(2, i))
+        if i < others:
+            late.append(lambda i=i: only(outer, lambda: from_z(3, i)))
+    early += [lambda i=i: only(inner, lambda: from_z(3, i)) for i in range(3, chips)]
+    for j, items in ((yi, early), (1 - yi, late)):
+        if items is late:
+            from_y(1, others)
+            pair_wait(2)
+            queries(j)
+            from_y(2, 1)
+        parts = [(own, turn) for own in (False, True) for turn in range(turns)]
+        for n, (own, turn) in enumerate(parts):
+            attend(own, j, turn)
+            if not own:
+                give(j, turn)
+            for item in items[n * len(items) // len(parts):(n + 1) * len(items) // len(parts)]:
+                item()
 
     def project(zones, mine):
         half = xi if mine else 1 - xi
-        left = att[half]
-        deep = pl.ds(pl.multiple_of(half * width, width), width)
         for at in zones:
-            part = jnp.dot(left, wob[deep, at], preferred_element_type=jnp.float32)
-            total[:, at] = part if mine else total[:, at] + part
+            part = None if mine else total[:, at]
+            for j in range(2):
+                deep = pl.ds(pl.multiple_of((half * 2 + j) * q_width, q_width), q_width)
+                term = jnp.dot(att[half, j], wob[deep, at], preferred_element_type=jnp.float32)
+                part = term if part is None else part + term
+            total[:, at] = part
 
     def zone(who):
         return pl.ds(pl.multiple_of(who * wide, 128), wide)
 
+    def corners(i):
+        corner_y(i)
+        corner_x(i)
+
     arrived(wob.at[rows(z, 1 - core)], own_recv, 0)
+    def project_late(at, first, stop):
+        part = total[:, at] if first else None
+        for owner in owners[first:stop]:
+            deep = pl.ds(pl.multiple_of(owner * q_width, q_width), q_width)
+            term = jnp.dot(att[owner // 2, owner % 2], wob[deep, at], preferred_element_type=jnp.float32)
+            part = term if part is None else part + term
+        total[:, at] = part
+
     pair_wait(3)
     pair_wait(4)
     project([zone(sp), zone(x_peer)], True)
+    corners(1)
+    arrived(att.at[1 - xi], att_recv, 0)
+    project([zone(sp), zone(x_peer)], False)
+    for i in range(2, others):
+        corners(i)
     pair_wait(5)
+    project([zone(y_peer)], True)
+    project([zone(y_peer)], False)
     pair_wait(7)
-    project([zone(y_peer), pl.ds(OD - rest, rest)], True)
-    for i in range(1, chips):
-        corner_y(i)
-        corner_x(i)
-    arrived(att.at[1 - xi], att_recv, 0)
-    project([pl.ds(OD - rest, rest), zone(sp), zone(x_peer), zone(y_peer)], False)
+    corners(others)
+    only(outer, lambda: from_z(3, others))
+    project_late(slice(OD - rest, OD), 0, others)
     pair_wait(6)
-    late = [zone(corner), pl.ds(4 * wide, 4 * narrow)]
-    project(late, True)
-    project(late, False)
-
-    chunk = R // 4
-    stores = []
-    for n in range(4):
-        at = pl.ds(n * chunk, chunk)
-        x = total[at]
-        scale = lax.rsqrt(jnp.mean(x * x, axis=-1, keepdims=True) + EPS)
-        out[at] = (x * scale * og_ref[...]).astype(jnp.bfloat16)
-        store = pltpu.make_async_copy(out.at[at], o_ref.at[at], load_sem.at[n])
-        store.start()
-        stores.append(store)
+    project_late(slice(4 * wide, OD - rest), 0, others)
+    project_late(zone(corner), 0, others)
+    pair_wait(9)
+    project_late(zone(corner), others, chips)
+    pair_wait(8)
+    project_late(slice(4 * wide, OD), others, chips)
 
     count = others * depth
     sent(x_ref, tok_send, 0)
@@ -813,7 +843,7 @@
     sent(quarters(others, 1, 2), y_send, 3)
     sent(quarters(others), x_send, 0)
     sent(quarters(others, 0, 1), x_send, 1)
-    sent(kv_buf.at[:2 * R], kv_send, 0)
+    sent(kv_buf.at[:, :2 * R], kv_send, 0)
     sent(att.at[2], att_send, 0)
     for group, ref in enumerate(pair_refs()):
         sent(ref, p_send, group)
@@ -838,8 +868,31 @@
                 ref = bulk(t)
                 remote(ref, ref, z_send.at[t, owner], z_recv.at[t, owner], peer).wait_send()
 
-    for store in stores:
-        store.wait()
+
+def rows_kernel(total, gain, o_ref, out, sem):
+    R = total.shape[0]
+    chunk = R // 4
+    for n in range(4):
+        at = pl.ds(n * chunk, chunk)
+        x = total[at]
+        scale = lax.rsqrt(jnp.mean(x * x, axis=-1, keepdims=True) + EPS)
+        out[at] = (x * scale * gain[...]).astype(jnp.bfloat16)
+        pltpu.make_async_copy(out.at[at], o_ref.at[at], sem).start()
+    pltpu.make_async_copy(out, o_ref, sem).wait()
+
+
+def finish_rows(total, gain):
+    vmem = pl.BlockSpec(memory_space=pltpu.VMEM)
+    return pl.pallas_call(
+        rows_kernel,
+        out_shape=jax.ShapeDtypeStruct(total.shape, jnp.bfloat16),
+        in_specs=[vmem, vmem],
+        out_specs=ANY,
+        scratch_shapes=[pltpu.VMEM(total.shape, jnp.bfloat16), pltpu.SemaphoreType.DMA],
+        compiler_params=pltpu.CompilerParams(vmem_limit_bytes=8 * 1024 * 1024),
+        cost_estimate=pl.CostEstimate(flops=4_000_000, bytes_accessed=2_000_000, transcendentals=0),
+        name="finish_rows",
+    )(total, gain[None])
 
 
 def fused(sequence, in_gain, query_weight, key_weight, value_matrix, query_gain, key_gain,
@@ -849,38 +902,36 @@
     columns = out_weight.shape[1]
     dma = pltpu.SemaphoreType.DMA
     bf16, f32 = jnp.bfloat16, jnp.float32
-    return pl.pallas_call(
+    total = pl.pallas_call(
         functools.partial(fused_kernel, chips, q_width, kv_width),
-        out_shape=jax.ShapeDtypeStruct((row_count, columns), bf16),
-        in_specs=[ANY] * 11,
-        out_specs=ANY,
+        out_shape=pltpu.VMEM((row_count, columns), f32),
+        in_specs=[pl.BlockSpec(memory_space=pltpu.HBM)] * 10,
+        out_specs=pl.BlockSpec(memory_space=pltpu.VMEM),
         scratch_shapes=[
             pltpu.VMEM((row_count, features), bf16),
             pltpu.VMEM((1, features), f32),
             pltpu.VMEM((1, HEAD_WIDTH), f32),
             pltpu.VMEM((1, HEAD_WIDTH), f32),
-            pltpu.VMEM((1, columns), f32),
             pltpu.VMEM((2 * row_count, features), bf16),
             pltpu.VMEM((2, features, 2 * kv_width), bf16),
             pltpu.VMEM((2, features, q_width), bf16),
             pltpu.VMEM((out_weight.shape[0] * chips * 2, columns), bf16),
-            pltpu.VMEM((2 * row_count, 2 * q_width), bf16),
-            pltpu.VMEM((4 * row_count, 4 * kv_width), bf16),
-            pltpu.VMEM((3, row_count, 2 * q_width), bf16),
-            pltpu.VMEM((row_count, columns), f32),
-            pltpu.VMEM((row_count, columns), bf16),
+            pltpu.VMEM((2, 2 * row_count, q_width), bf16),
+            pltpu.VMEM((2, 4 * row_count, 2 * kv_width), bf16),
+            pltpu.VMEM((3, 2, row_count, q_width), bf16),
             pltpu.VMEM((2 * row_count, HEAD_WIDTH), f32),
             pltpu.VMEM((2 * row_count, HEAD_WIDTH), f32),
             dma((14,)), dma((1,)), dma((1,)), dma((4, 2)), dma((4, chips)), dma((4, chips)),
             dma((4,)), dma((4, chips)), dma((2,)), dma((2, chips)),
-            dma((1,)), dma((2,)), dma((1,)), dma((1,)), dma((8,)), dma((8,)), dma((1,)), dma((1,)),
+            dma((1,)), dma((2,)), dma((1,)), dma((1,)), dma((10,)), dma((10,)), dma((1,)), dma((1,)),
         ],
         compiler_params=pltpu.CompilerParams(
-            collective_id=0, has_side_effects=True, vmem_limit_bytes=60 * 1024 * 1024),
+            collective_id=0, has_side_effects=True, vmem_limit_bytes=56 * 1024 * 1024),
         cost_estimate=pl.CostEstimate(flops=10_000_000_000, bytes_accessed=10_000_000, transcendentals=0),
         name="attention_layer",
     )(sequence, query_weight, key_weight, value_matrix, out_weight, in_gain[None], query_gain[None],
-      key_gain[None], cosine, sine, out_gain[None])
+      key_gain[None], cosine, sine)
+    return finish_rows(total, out_gain)
 
 
 def rotation(length):
@@ -913,7 +964,7 @@
     kv_heads = max(1, KEY_VALUE_HEADS // parts)
     per_group = QUERY_HEAD_COUNT // KEY_VALUE_HEADS
     cosine, sine = rotation(parts * row_count)
-    if parts == 4:
+    if parts == 4 and groups == 8:
         return fused(sequence, in_gain, query_weight, key_weight, value_matrix, query_gain, key_gain,
                      out_weight, out_gain, cosine, sine, groups // 2)[None]
     rows, columns, out_head, own_tail = gather(

time: 77 us -> 72.2 us (0.938)
  Pallas kernels: 74.3 us -> 71.1 us
  local copies, waits for them, and re-layouts: 2.3 us -> 0.01 us
    pallas_call x1, Pallas kernels: 74.3 us -> 70 us  [fused(): pl.pallas_call(functools.partial(fused_kernel, chips, q_width, kv_width),...]
    unnamed x1 -> x2, local copies, waits for them, and re-layouts: 2.3 us -> 0.01 us
    pallas_call x0 -> x1, Pallas kernels: none -> 1.15 us  [finish_rows(): pl.pallas_call(rows_kernel, out_shape=jax.ShapeDtypeStruct(total.shape, j...]
where the time goes in v3:
time: 72.2 us; the launch traced here: 71.3 us
  Pallas kernels  71.1 us (98%)
    pallas_call x1, Pallas kernels, fused(): pl.pallas_call(functools.partial(fused_kernel, chips, q_width, kv_width),...  70 us

profile of v3, /device:TPU:1, one launch (start us, length us, event | category | flops | bytes accessed | tf_op | source)
XLA Modules:
  0.0 71.3 jit_solution(13638357517087617390)
XLA Ops:
  0.0 0.0 copy-start
  0.0 70.0 %attention_layer.1.total = f32[256,2048]{1,0:T(8,128)S(1)} custom-call(bf16[256,2048]{1,0:T(8,128)(2,1)} %bitcast.7, bf16[256,2048]{1,0:T(8,128)(2,1)} %wq_ref.1, bf16[256,512]{1,0:T(8,128)(2,1)} %wk_ref.1, bf16[256,512]{1,0:T(8,128)(2,1)} %wv_ref.1, bf16[256,2048]{1,0:T(8,128)(2,1)} %wo_ref.1, f32[1,2048]{1,0:T(1,128)} %bitcast.8, f32[1,128]{1,0:T(1,128)} %bitcast.9, ...), custom_call_target="tpu_custom_call" | custom-call | flops 10000000000 | bytes 10000000 | tf_op jit(solution)/shard_map/attention_layer/pallas_call | solution.py:905
  70.0 0.0 copy-done
  70.0 1.2 %finish_rows.1 = bf16[256,2048]{1,0:T(8,128)(2,1)} custom-call(f32[256,2048]{1,0:T(8,128)S(1)} %attention_layer.1.total, f32[1,2048]{1,0:T(1,128)S(1)} %bitcast.6), custom_call_target="tpu_custom_call" | custom-call | flops 4000000 | bytes 2000000 | tf_op jit(solution)/shard_map/finish_rows/pallas_call | solution.py:886
Async XLA Ops:
  0.0 70.0 %copy-start = (f32[2048]{0:T(1024)S(1)}, f32[2048]{0:T(1024)}, u32[]{:S(2)}) copy-start(f32[2048]{0:T(1024)} %param.19) | copy-start | bytes 24580
